TPU v7x, 32 devices: a whole 2x2x4 slice. The times are simulated.
32 devices in a mesh: grp: 2 (over y), fs: 4 (over z), tp: 4 (over x, core).
Axes of the slice: x: 2, y: 2, z: 4, core: 2. Of those that a mesh axis runs over, the one named last changes fastest.
Arguments:
- tokens: bfloat16 [8, 384, 2048], P(('grp', 'fs'), None, 'tp'), parts along dimension 0, may hold values from -24 to 24
- input_gain: float32 [2048], replicated, may hold values from 0.1 to 1.9
- query_weight: bfloat16 [2048, 1024], P('fs', 'tp'), may hold values from -0.125 to 0.125
- key_weight: bfloat16 [2048, 1024], P('fs', 'tp'), may hold values from -0.125 to 0.125
- value_weight: bfloat16 [2048, 1024], P('fs', 'tp'), may hold values from -0.125 to 0.125
- output_gate_matrix: bfloat16 [2048, 1024], P('fs', 'tp'), may hold values from -0.125 to 0.125
- forward_decay: float32 [16], P('tp'), may hold values from -1 to 9
- backward_decay: float32 [16], P('tp'), may hold values from -1 to 9
- merge_weight: bfloat16 [1024, 2048], P('tp', 'fs'), may hold values from -0.375 to 0.375
- middle_gain: float32 [2048], replicated, may hold values from 0.1 to 1.9
- gate_weight: bfloat16 [2048, 5120], P('fs', 'tp'), may hold values from -0.125 to 0.125
- up_weight: bfloat16 [2048, 5120], P('fs', 'tp'), may hold values from -0.125 to 0.125
- down_weight: bfloat16 [5120, 2048], P('tp', 'fs'), may hold values from -0.15625 to 0.15625
Outputs:
- layer_out: bfloat16 [8, 384, 2048], P(('grp', 'fs'), None, 'tp'), parts along dimension 0
There are 2 independent parts, one for each index of `grp`. A program takes and returns all parts, laid end to end along the dimension named above; an argument that names none is the same for every part. Nothing has to cross between parts.
All inputs are finite; a program needn't handle non-finite values.
Results may differ from a plain program's by a relative error of at most 0.019.
Values may be sent and summed in bfloat16 or wider, within the bound.
A program may use at most 64 MiB of HBM per device.

v0:
```python
import functools

import jax
import jax.numpy as jnp
import numpy as np
from jax import lax
from jax.experimental import pallas as pl
from jax.experimental.pallas import tpu as pltpu
from jax.sharding import PartitionSpec as P

norm_eps = 1e-06
group_eps = 1e-05
rope_base = 10000.0


def turn_tables(length, head_dim, head_count):
    half_dim = head_dim // 2
    inverse = rope_base ** (-np.arange(half_dim) / half_dim)
    angles = np.arange(length)[:, None] * inverse[None, :]
    cosine, sine_part = np.cos(angles), np.sin(angles)
    return (
        np.tile(np.concatenate([cosine, cosine], axis=1), (1, head_count)).astype(np.float32),
        np.tile(np.concatenate([-sine_part, sine_part], axis=1), (1, head_count)).astype(np.float32),
    )


MESH = pl.DeviceIdType.MESH


def layer_kernel(
    sizes,
    tokens,
    input_gain,
    middle_gain,
    rate_ahead,
    rate_behind,
    cosine,
    sine_part,
    joined_shard,
    merge_shard,
    gate_shard,
    up_shard,
    down_shard,
    out,
    joined,
    merge,
    gate,
    up,
    *rest,
):
    line, copies, row = sizes["fs"], sizes["grp"], sizes["tp"]
    parts = len(rest) - 18
    downs, partial_ends, received_ends = rest[:parts], rest[-2], rest[-1]
    (
        gathered,
        gathered_mid,
        normed,
        projected,
        mixed,
        hidden,
        partial,
        received,
        own_sem,
        line_send,
        line_recv,
        pair_send,
        pair_recv,
        row_send,
        row_recv,
        self_sem,
    ) = rest[parts:-2]
    piece_width = downs[0].shape[2]
    shards = (joined_shard, merge_shard, gate_shard, up_shard) + tuple(
        down_shard if parts == 1 else down_shard.at[:, pl.ds(i * piece_width, piece_width)]
        for i in range(parts)
    )
    slots = (joined, merge, gate, up) + tuple(downs)
    count = len(slots)
    length, part_width = tokens.shape
    width = row * part_width
    seat = lax.axis_index("tp")
    place = lax.axis_index("fs")
    half = lax.axis_index("grp")

    barrier = pltpu.get_barrier_semaphore()
    for shift in (1, -1):
        there = place + shift

        @pl.when((there >= 0) & (there < line))
        def _():
            pl.semaphore_signal(barrier, inc=1, device_id={"fs": there}, device_id_type=MESH)

    for other in range(1, copies):
        pl.semaphore_signal(
            barrier,
            inc=1,
            device_id={"grp": lax.rem(half + other, copies)},
            device_id_type=MESH,
        )
    for other in range(1, row):
        pl.semaphore_signal(
            barrier,
            inc=1,
            device_id={"tp": lax.rem(seat + other, row)},
            device_id_type=MESH,
        )
    own = [pltpu.make_async_copy(shards[k], slots[k].at[place], own_sem.at[k]) for k in range(count)]
    for copy in own:
        copy.start()
    neighbours = (place > 0).astype(jnp.int32) + (place < line - 1).astype(jnp.int32)
    mine = pltpu.make_async_copy(tokens, gathered.at[seat], self_sem)
    mine.start()
    pl.semaphore_wait(barrier, neighbours + copies - 1 + row - 1)

    def piece(k, block, part):
        rows = slots[k].shape[1] // copies
        return slots[k].at[block, pl.ds(pl.multiple_of(part * rows, rows), rows), :]

    def hop(k, way, step):
        shift = 1 if way == 0 else -1
        block = place - shift * step
        return pltpu.make_async_remote_copy(
            src_ref=piece(k, block, half),
            dst_ref=piece(k, block, half),
            send_sem=line_send.at[k, way, step],
            recv_sem=line_recv.at[k, way, step],
            device_id={"fs": place + shift},
            device_id_type=MESH,
        )

    def arrival(k, way, step):
        shift = 1 if way == 0 else -1
        block = place - shift * step
        return pltpu.make_async_remote_copy(
            src_ref=piece(k, block, half),
            dst_ref=piece(k, block, half),
            send_sem=line_send.at[k, way, step - 1],
            recv_sem=line_recv.at[k, way, step - 1],
            device_id={"fs": place - shift},
            device_id_type=MESH,
        )

    def across(k, way, step, other):
        shift = 1 if way == 0 else -1
        block = place - shift * step
        return pltpu.make_async_remote_copy(
            src_ref=piece(k, block, half),
            dst_ref=piece(k, block, half),
            send_sem=pair_send.at[k, way, step - 1, other - 1],
            recv_sem=pair_recv.at[k, way, step - 1, other - 1],
            device_id={"grp": lax.rem(half + other, copies)},
            device_id_type=MESH,
        )

    def landed(k, way, step, other):
        shift = 1 if way == 0 else -1
        block = place - shift * step
        source = lax.rem(half + copies - other, copies)
        return pltpu.make_async_remote_copy(
            src_ref=piece(k, block, source),
            dst_ref=piece(k, block, source),
            send_sem=pair_send.at[k, way, step - 1, other - 1],
            recv_sem=pair_recv.at[k, way, step - 1, other - 1],
            device_id={"grp": source},
            device_id_type=MESH,
        )

    def has(way, step):
        return place >= step if way == 0 else place + step < line

    def goes(way):
        return place < line - 1 if way == 0 else place > 0

    def launch(k):
        own[k].wait()
        for way in range(2):

            @pl.when(goes(way))
            def _():
                hop(k, way, 0).start()

    def pump(k):
        for step in range(1, line):
            for way in range(2):

                @pl.when(has(way, step))
                def _():
                    arrival(k, way, step).wait_recv()
                    for other in range(1, copies):
                        across(k, way, step, other).start()

                @pl.when(has(way, step) & goes(way))
                def _():
                    hop(k, way, step).start()

    def settle(k):
        for step in range(1, line):
            for way in range(2):

                @pl.when(has(way, step))
                def _():
                    for other in range(1, copies):
                        landed(k, way, step, other).wait_recv()

    def drain(k):
        for way in range(2):
            for step in range(line):

                @pl.when((has(way, step) if step else True) & goes(way))
                def _():
                    hop(k, way, step).wait_send()

                if step:

                    @pl.when(has(way, step))
                    def _():
                        for other in range(1, copies):
                            across(k, way, step, other).wait_send()

    def spread(source, target, stage):
        return [
            pltpu.make_async_remote_copy(
                src_ref=source,
                dst_ref=target.at[seat],
                send_sem=row_send.at[stage, other - 1],
                recv_sem=row_recv.at[stage, other - 1],
                device_id={"tp": lax.rem(seat + other, row)},
                device_id_type=MESH,
            )
            for other in range(1, row)
        ]

    def spread_in(target, stage):
        sources = [lax.rem(seat + row - other, row) for other in range(1, row)]
        return [
            pltpu.make_async_remote_copy(
                src_ref=target.at[source],
                dst_ref=target.at[source],
                send_sem=row_send.at[stage, other],
                recv_sem=row_recv.at[stage, other],
                device_id={"tp": source},
                device_id_type=MESH,
            )
            for other, source in enumerate(sources)
        ]

    def scatter(source, target, stage, other):
        there = lax.rem(seat + other, row)
        return pltpu.make_async_remote_copy(
            src_ref=source.at[there],
            dst_ref=target.at[other - 1],
            send_sem=row_send.at[stage, other - 1],
            recv_sem=row_recv.at[stage, other - 1],
            device_id={"tp": there},
            device_id_type=MESH,
        )

    def normalize(source, gain_vector):
        total = jnp.zeros((length, 1), jnp.float32)
        for t in range(row):
            widened = source[t].astype(jnp.float32)
            total = total + jnp.sum(widened * widened, axis=1, keepdims=True)
        scale = lax.rsqrt(total / width + norm_eps)
        for t in range(row):
            span = slice(t * part_width, (t + 1) * part_width)
            scaled = source[t].astype(jnp.float32) * scale * gain_vector[:, span]
            normed[:, span] = scaled.astype(jnp.bfloat16)

    def times(weight, columns):
        block = weight[:, :, columns]
        return jnp.dot(
            normed[...], block.reshape(-1, block.shape[2]), preferred_element_type=jnp.float32
        )

    def shares(rows_in, weight, target):
        step = weight.shape[2]
        for block in range(line):
            term = jnp.dot(rows_in[...], weight[block], preferred_element_type=jnp.float32)
            begin = block * step
            inner = begin % part_width
            target[begin // part_width, :, inner : inner + step] = term.astype(jnp.bfloat16)

    def finish(i):
        settle(4 + i)
        if parts == 1:
            shares(hidden, downs[i], partial_ends.at[i])
        else:
            for j in range(row):
                blocks = [jnp.dot(
                    hidden[...], downs[i][j * line // row + c], preferred_element_type=jnp.float32
                ) for c in range(max(1, line // row))]
                for c, term in enumerate(blocks):
                    partial_ends[i, j, :, c * piece_width : (c + 1) * piece_width] = term.astype(
                        jnp.bfloat16
                    )
        for other in range(1, row):
            scatter(partial_ends.at[i], received_ends.at[i], 3 + i, other).start()

    def collect(i):
        span = slice(None) if parts == 1 else slice(i * piece_width, (i + 1) * piece_width)
        total = gathered_mid[seat, :, span].astype(jnp.float32)
        total = total + partial_ends[i, seat].astype(jnp.float32)
        for other in range(1, row):
            scatter(partial_ends.at[i], received_ends.at[i], 3 + i, other).wait_recv()
            total = total + received_ends[i, other - 1].astype(jnp.float32)
        out[:, span] = total.astype(jnp.bfloat16)

    launch(0)
    first = spread(tokens, gathered, 0)
    for copy in first:
        copy.start()
    launch(1)
    mine.wait()
    for copy in spread_in(gathered, 0):
        copy.wait_recv()
    normalize(gathered, input_gain)

    pump(0)
    launch(2)
    settle(0)
    ret_width = projected.shape[2]
    for t in range(4):
        projected[t] = (
            times(joined, slice(t * ret_width, (t + 1) * ret_width))
            .astype(jnp.bfloat16)
            .astype(jnp.float32)
        )
    pump(1)
    launch(3)

    head_count = rate_ahead.shape[0]
    head_dim = ret_width // head_count
    lane = lax.broadcasted_iota(jnp.int32, (length, ret_width), 1)
    in_lower = lax.rem(lane, head_dim) < head_dim // 2

    def turned(values):
        partner = jnp.where(
            in_lower,
            pltpu.roll(values, ret_width - head_dim // 2, 1),
            pltpu.roll(values, head_dim // 2, 1),
        )
        return values * cosine[...] + partner * sine_part[...]

    queries = turned(projected[0])
    key_heads = (turned(projected[1]) * head_dim ** (-0.5)).astype(jnp.bfloat16)
    valued = projected[2]
    offset = (
        lax.broadcasted_iota(jnp.int32, (length, length), 0)
        - lax.broadcasted_iota(jnp.int32, (length, length), 1)
    ).astype(jnp.float32)
    result = jnp.zeros((length, ret_width), jnp.float32)
    for h in range(head_count):
        here = (lane >= h * head_dim) & (lane < (h + 1) * head_dim)
        scores = lax.dot_general(
            jnp.where(here, queries, 0.0).astype(jnp.bfloat16),
            key_heads,
            (((1,), (1,)), ((), ())),
            preferred_element_type=jnp.float32,
        )
        decay = jnp.exp(jnp.where(offset >= 0, rate_ahead[h] * offset, -rate_behind[h] * offset))
        result = result + jnp.dot(
            (scores * decay).astype(jnp.bfloat16),
            jnp.where(here, valued, 0.0).astype(jnp.bfloat16),
            preferred_element_type=jnp.float32,
        )
    center = jnp.zeros((length, ret_width), jnp.float32)
    for h in range(head_count):
        here = (lane >= h * head_dim) & (lane < (h + 1) * head_dim)
        mean = jnp.sum(jnp.where(here, result, 0.0), axis=1, keepdims=True) / head_dim
        center = jnp.where(here, mean, center)
    centered = result - center
    squared = centered * centered
    factor = jnp.zeros((length, ret_width), jnp.float32)
    for h in range(head_count):
        here = (lane >= h * head_dim) & (lane < (h + 1) * head_dim)
        spread_h = jnp.sum(jnp.where(here, squared, 0.0), axis=1, keepdims=True) / head_dim
        factor = jnp.where(here, lax.rsqrt(spread_h + group_eps), factor)
    gates = projected[3]
    mixed[...] = (gates / (1.0 + jnp.exp(-gates)) * (centered * factor)).astype(jnp.bfloat16)

    settle(1)
    shares(mixed, merge, partial)
    for other in range(1, row):
        scatter(partial, received, 1, other).start()
    pump(2)
    total = tokens[...].astype(jnp.float32) + partial[seat].astype(jnp.float32)
    for other in range(1, row):
        scatter(partial, received, 1, other).wait_recv()
        total = total + received[other - 1].astype(jnp.float32)
    gathered_mid[seat] = total.astype(jnp.bfloat16)
    second = spread(gathered_mid.at[seat], gathered_mid, 2)
    for copy in second:
        copy.start()
    pump(3)
    launch(4)
    if parts > 1:
        launch(5)
    for copy in spread_in(gathered_mid, 2):
        copy.wait_recv()
    normalize(gathered_mid, middle_gain)
    settle(2)
    settle(3)
    hidden_width = hidden.shape[1]
    tile = 256 if hidden_width % 256 == 0 else 128

    @pl.loop(0, hidden_width // tile)
    def _(index):
        columns = pl.ds(pl.multiple_of(index * tile, tile), tile)
        gate_act = times(gate, columns)
        up_act = times(up, columns)
        hidden[:, columns] = (gate_act / (1.0 + jnp.exp(-gate_act)) * up_act).astype(jnp.bfloat16)

    for i in range(parts):
        pump(4 + i)
        if i + 2 < parts:
            launch(6 + i)
        if i:
            finish(i - 1)
    finish(parts - 1)
    for i in range(parts):
        collect(i)
    for copy in first + second:
        copy.wait_send()
    for other in range(1, row):
        scatter(partial, received, 1, other).wait_send()
        for i in range(parts):
            scatter(partial_ends.at[i], received_ends.at[i], 3 + i, other).wait_send()
    for k in range(count):
        drain(k)


def on_device(
    sizes,
    tokens,
    input_gain,
    query_weight,
    key_weight,
    value_weight,
    output_gate_matrix,
    forward_decay,
    backward_decay,
    merge_weight,
    middle_gain,
    gate_weight,
    up_weight,
    down_weight,
):
    seq_count, length, part_width = tokens.shape
    flat = tokens.reshape(seq_count * length, part_width)
    joined = jnp.concatenate([query_weight, key_weight, value_weight, output_gate_matrix], axis=1)
    shards = (joined, merge_weight, gate_weight, up_weight, down_weight)
    line, copies, row = sizes["fs"], sizes["grp"], sizes["tp"]
    down_width = down_weight.shape[1]
    parts = down_width // 256 if line == row and down_width % 256 == 0 else 1
    down_piece = jax.ShapeDtypeStruct((down_weight.shape[0], down_width // parts), jnp.bfloat16)
    landing = shards[:4] + (down_piece,) * parts
    count = len(landing)
    width, ret_width, hidden_width = row * part_width, query_weight.shape[1], gate_weight.shape[1]
    head_count = forward_decay.shape[0]
    tables = turn_tables(length, ret_width // head_count, head_count)
    in_vmem = pl.BlockSpec(memory_space=pltpu.VMEM)
    in_smem = pl.BlockSpec(memory_space=pltpu.SMEM)
    bf16 = jnp.bfloat16
    layer_out = pl.pallas_call(
        functools.partial(layer_kernel, sizes),
        out_shape=jax.ShapeDtypeStruct(flat.shape, bf16),
        in_specs=[in_vmem] * 3
        + [in_smem] * 2
        + [in_vmem] * 2
        + [pl.BlockSpec(memory_space=pl.ANY)] * len(shards),
        out_specs=in_vmem,
        scratch_shapes=[pltpu.VMEM((line,) + w.shape, w.dtype) for w in landing]
        + [
            pltpu.VMEM((row, length, part_width), bf16),
            pltpu.VMEM((row, length, part_width), bf16),
            pltpu.VMEM((length, width), bf16),
            pltpu.VMEM((4, length, ret_width), jnp.float32),
            pltpu.VMEM((length, ret_width), bf16),
            pltpu.VMEM((length, hidden_width), bf16),
            pltpu.VMEM((row, length, part_width), bf16),
            pltpu.VMEM((row - 1, length, part_width), bf16),
            pltpu.SemaphoreType.DMA((count,)),
            pltpu.SemaphoreType.DMA((count, 2, line)),
            pltpu.SemaphoreType.DMA((count, 2, line)),
            pltpu.SemaphoreType.DMA((count, 2, line, copies - 1)),
            pltpu.SemaphoreType.DMA((count, 2, line, copies - 1)),
            pltpu.SemaphoreType.DMA((3 + parts, row - 1)),
            pltpu.SemaphoreType.DMA((3 + parts, row - 1)),
            pltpu.SemaphoreType.DMA,
            pltpu.VMEM((parts, row, length, part_width // parts), bf16),
            pltpu.VMEM((parts, row - 1, length, part_width // parts), bf16),
        ],
        compiler_params=pltpu.CompilerParams(
            collective_id=0, has_side_effects=True, vmem_limit_bytes=58 << 20
        ),
    )(
        flat,
        input_gain[None, :],
        middle_gain[None, :],
        jax.nn.log_sigmoid(forward_decay),
        jax.nn.log_sigmoid(backward_decay),
        *tables,
        *shards,
    )
    return layer_out.reshape(seq_count, length, part_width)


def solution(mesh):
    placed = (
        P(("grp", "fs"), None, "tp"),
        P(),
        P("fs", "tp"),
        P("fs", "tp"),
        P("fs", "tp"),
        P("fs", "tp"),
        P("tp"),
        P("tp"),
        P("tp", "fs"),
        P(),
        P("fs", "tp"),
        P("fs", "tp"),
        P("tp", "fs"),
    )
    return jax.shard_map(
        functools.partial(on_device, dict(mesh.shape)),
        mesh=mesh,
        in_specs=placed,
        out_specs=P(("grp", "fs"), None, "tp"),
        check_vma=False,
    )
```

profile of v0, /device:TPU:0, one launch (start us, length us, event | category | flops | bytes accessed | tf_op | source)
XLA Modules:
  0.0 218.1 jit_solution(5298518211976847505)
XLA Ops:
  0.0 1.3 fusion
  1.3 2.3 %pad_maximum_fusion.joined_shard = bf16[512,1024]{1,0:T(8,128)(2,1)} fusion(bf16[512,256]{1,0:T(8,128)(2,1)} %param.20, bf16[512,256]{1,0:T(8,128)(2,1)} %param.19, bf16[512,256]{1,0:T(8,128)(2,1)} %param.18, bf16[512,256]{1,0:T(8,128)(2,1)} %param.17), kind=kLoop, calls=%fused_computation | loop fusion | flops 4194304 | bytes 2097152 | tf_op jit(solution)/shard_map/concatenate | solution.py:450
  3.6 212.7 %shard_map.145 = bf16[384,512]{1,0:T(8,128)(2,1)} custom-call(bf16[384,512]{1,0:T(8,128)(2,1)} %bitcast.5, f32[1,2048]{1,0:T(1,128)} %bitcast.6, f32[1,2048]{1,0:T(1,128)} %bitcast.7, f32[4]{0:T(128)} %get-tuple-element.5.rate_ahead, f32[4]{0:T(128)} %get-tuple-element.6.rate_behind, f32[384,256]{1,0:T(8,128)} %constant.9.clone.cosine, ...), custom_call_target="tpu_custom_call" | custom-call | tf_op jit(solution)/shard_map/pallas_call | solution.py:464
  216.3 1.8 copy.17
where the time goes:
time: 220 us; the launch traced here: 218 us
  Pallas kernels  213 us (97%)
  other arithmetic  3.59 us (2%)
    pallas_call x1, Pallas kernels, on_device(): pl.pallas_call(functools.partial(layer_kernel, sizes), out_shape=jax.Shap...  213 us

commit v1 on v0

--- a/solution.py
+++ b/solution.py
@@ -429,6 +429,565 @@
         drain(k)
 
 
+def paired_kernel(
+    sizes,
+    tokens,
+    input_gain,
+    middle_gain,
+    rate_ahead,
+    rate_behind,
+    cosine,
+    sine_part,
+    query_shard,
+    key_shard,
+    value_shard,
+    output_gate_shard,
+    merge_shard,
+    gate_shard,
+    up_shard,
+    down_shard,
+    out,
+    joined_out,
+    merge_out,
+    gate_out,
+    up_out,
+    down_out,
+    joined,
+    merge,
+    gate,
+    up,
+    down,
+    gathered,
+    gathered_mid,
+    normed,
+    projected,
+    mixed,
+    hidden,
+    first_partial,
+    first_core,
+    first_row,
+    first_line,
+    last_partial,
+    last_core,
+    last_row,
+    last_line,
+    own_sem,
+    line_send,
+    line_recv,
+    pair_send,
+    pair_recv,
+    share_send,
+    share_recv,
+    sum_send,
+    sum_recv,
+):
+    line, row = sizes["fs"], sizes["tp"]
+    pieces = down.shape[0]
+    piece_width = down.shape[3]
+    length, part_width = tokens.shape
+    width = row * part_width
+    seat = lax.axis_index("tp")
+    place = lax.axis_index("fs")
+    half = lax.axis_index("grp")
+    core, column = lax.rem(seat, 2), seat // 2
+    slot = lax.rem(place, 2)
+    core_peer = seat + 1 - 2 * core
+    row_peer = lax.rem(seat + 2, row)
+    far_peer = lax.rem(core_peer + 2, row)
+    line_peer = place + 1 - 2 * slot
+    sign = 1 - 2 * (place // (line // 2))
+    others = [lax.rem(place + sign * step + line, line) for step in range(1, line)]
+
+    barrier = pltpu.get_barrier_semaphore()
+    for there in others:
+        pl.semaphore_signal(barrier, inc=1, device_id={"fs": there}, device_id_type=MESH)
+    pl.semaphore_signal(barrier, inc=1, device_id={"grp": 1 - half}, device_id_type=MESH)
+    for there in (core_peer, row_peer):
+        pl.semaphore_signal(barrier, inc=1, device_id={"tp": there}, device_id_type=MESH)
+
+    group = joined_out.shape[2] // 4
+    quads = (query_shard, key_shard, value_shard, output_gate_shard)
+    merge_rows = merge.shape[1]
+    hidden_half = gate.shape[2]
+
+    def cut(ref, axis, part, size):
+        window = pl.ds(pl.multiple_of(part * size, size), size)
+        return ref.at[window] if axis == 0 else ref.at[:, window]
+
+    loads = [
+        [
+            (quad.at[:, p * group : (p + 1) * group], joined_out.at[p, :, i * group : (i + 1) * group])
+            for p in range(2)
+            for i, quad in enumerate(quads)
+        ],
+        [(merge_shard, merge_out)],
+        [(gate_shard, gate_out)],
+        [(up_shard, up_out)],
+        [(down_shard, down_out)],
+        [
+            (cut(quad, 1, slot, group), joined.at[place, :, i * group : (i + 1) * group])
+            for i, quad in enumerate(quads)
+        ],
+        [(cut(merge_shard, 0, slot, merge_rows), merge.at[place])],
+        [(cut(gate_shard, 1, slot, hidden_half), gate.at[place])],
+        [(cut(up_shard, 1, slot, hidden_half), up.at[place])],
+        [
+            (
+                cut(down_shard, 0, slot, hidden_half).at[:, i * piece_width : (i + 1) * piece_width],
+                down.at[i, place],
+            )
+            for i in range(pieces)
+        ],
+    ]
+    own, index = [], 0
+    for pairs in loads:
+        own.append([])
+        for source, target in pairs:
+            own[-1].append(pltpu.make_async_copy(source, target, own_sem.at[index]))
+            index += 1
+    for copies in own:
+        for copy in copies:
+            copy.start()
+    gathered[slot, seat] = tokens[...]
+    pl.semaphore_wait(barrier, line - 1 + 1 + 2)
+
+    def ready(k):
+        for copy in own[k]:
+            copy.wait()
+
+    def outgoing(k, parity):
+        if k == 0:
+            size = joined.shape[1] // 2
+            return joined_out.at[parity, pl.ds(pl.multiple_of(half * size, size), size)]
+        if k == 1:
+            size = merge_rows // 2
+            return cut(merge_out, 0, parity * 2 + half, size)
+        if k < 4:
+            source = (gate_out, up_out)[k - 2]
+            size = source.shape[0] // 2
+            return cut(source, 0, half, size).at[
+                :, pl.ds(pl.multiple_of(parity * hidden_half, hidden_half), hidden_half)
+            ]
+        size = hidden_half // 2
+        return cut(down_out, 0, parity * 2 + half, size).at[
+            :, (k - 4) * piece_width : (k - 3) * piece_width
+        ]
+
+    def landing(k, block, part):
+        target = (joined, merge, gate, up)[k] if k < 4 else down.at[k - 4]
+        size = target.shape[1] // 2
+        return target.at[block, pl.ds(pl.multiple_of(part * size, size), size)]
+
+    def post(k, there):
+        return pltpu.make_async_remote_copy(
+            src_ref=outgoing(k, lax.rem(there, 2)),
+            dst_ref=landing(k, place, half),
+            send_sem=line_send.at[k, there],
+            recv_sem=line_recv.at[k, place],
+            device_id={"fs": there},
+            device_id_type=MESH,
+        )
+
+    def arrival(k, block):
+        return pltpu.make_async_remote_copy(
+            src_ref=landing(k, block, half),
+            dst_ref=landing(k, block, half),
+            send_sem=line_send.at[k, block],
+            recv_sem=line_recv.at[k, block],
+            device_id={"fs": block},
+            device_id_type=MESH,
+        )
+
+    def across(k, block, part):
+        return pltpu.make_async_remote_copy(
+            src_ref=landing(k, block, part),
+            dst_ref=landing(k, block, part),
+            send_sem=pair_send.at[k, block],
+            recv_sem=pair_recv.at[k, block],
+            device_id={"grp": 1 - half},
+            device_id_type=MESH,
+        )
+
+    def launch(k):
+        ready(k)
+        for there in others:
+            post(k, there).start()
+
+    def pump(k, block):
+        arrival(k, block).wait_recv()
+        across(k, block, half).start()
+
+    def settle(k):
+        for block in others:
+            across(k, block, 1 - half).wait_recv()
+
+    def handed(source, target, stage, step):
+        plane = slot if step in (0, 1, 2, 3) else 1 - slot
+        holder = seat if step in (0, 1, 2, 4, 5) else row_peer
+        place_in = target.at[plane, holder]
+        peer = {"tp": core_peer}
+        if step in (1, 5):
+            peer = {"tp": row_peer}
+        if step == 2:
+            peer = {"fs": line_peer}
+        return pltpu.make_async_remote_copy(
+            src_ref=source if step < 3 else place_in,
+            dst_ref=place_in,
+            send_sem=share_send.at[stage, step],
+            recv_sem=share_recv.at[stage, step],
+            device_id=peer,
+            device_id_type=MESH,
+        )
+
+    def received(target, stage, step):
+        plane = slot if step in (0, 1, 3) else 1 - slot
+        holder = (core_peer, row_peer, seat, far_peer, core_peer, row_peer, far_peer)[step]
+        place_in = target.at[plane, holder]
+        return pltpu.make_async_remote_copy(
+            src_ref=place_in,
+            dst_ref=place_in,
+            send_sem=share_send.at[stage, step],
+            recv_sem=share_recv.at[stage, step],
+            device_id={"tp": core_peer},
+            device_id_type=MESH,
+        )
+
+    def normalize(source, gain_vector, plane):
+        total = jnp.zeros((length, 1), jnp.float32)
+        for t in range(row):
+            widened = source[plane, t].astype(jnp.float32)
+            total = total + jnp.sum(widened * widened, axis=1, keepdims=True)
+        scale = lax.rsqrt(total / width + norm_eps)
+        for t in range(row):
+            span = slice(t * part_width, (t + 1) * part_width)
+            scaled = source[plane, t].astype(jnp.float32) * scale * gain_vector[:, span]
+            normed[plane, :, span] = scaled.astype(jnp.bfloat16)
+
+    def hand_over(source, target, stage):
+        return [handed(source, target, stage, step) for step in range(7)]
+
+    def moved(source, target, peer, stage, step):
+        return pltpu.make_async_remote_copy(
+            src_ref=source,
+            dst_ref=target,
+            send_sem=sum_send.at[stage, step],
+            recv_sem=sum_recv.at[stage, step],
+            device_id=peer,
+            device_id_type=MESH,
+        )
+
+    def reducer(partial, core_in, row_in, line_in, stage):
+        return [
+            moved(partial.at[1 - core], core_in, {"tp": core_peer}, stage, 0),
+            moved(partial.at[core, 1 - column, 1 - slot], row_in.at[0], {"tp": row_peer}, stage, 1),
+            moved(partial.at[core, 1 - column, slot], row_in.at[1], {"tp": row_peer}, stage, 2),
+            moved(partial.at[core, column, 1 - slot], line_in, {"fs": line_peer}, stage, 3),
+        ]
+
+    def add_core(partial, core_in, steps):
+        steps[0].wait_recv()
+        for step, plane in ((1, 1 - slot), (2, slot)):
+            total = partial[core, 1 - column, plane].astype(jnp.float32) + core_in[
+                1 - column, plane
+            ].astype(jnp.float32)
+            partial[core, 1 - column, plane] = total.astype(jnp.bfloat16)
+            steps[step].start()
+
+    def add_row(partial, core_in, row_in, steps, step):
+        plane = 1 - slot if step == 1 else slot
+        steps[step].wait_recv()
+        return (
+            partial[core, column, plane].astype(jnp.float32)
+            + core_in[column, plane].astype(jnp.float32)
+            + row_in[step - 1].astype(jnp.float32)
+        )
+
+    def pass_line(partial, core_in, row_in, steps):
+        total = add_row(partial, core_in, row_in, steps, 1)
+        partial[core, column, 1 - slot] = total.astype(jnp.bfloat16)
+        steps[3].start()
+
+    first = hand_over(tokens, gathered, 0)
+    for step in (2, 1, 0):
+        first[step].start()
+    launch(0)
+    launch(1)
+    launch(2)
+    received(gathered, 0, 1).wait_recv()
+    first[3].start()
+    received(gathered, 0, 2).wait_recv()
+    first[5].start()
+    first[4].start()
+    received(gathered, 0, 0).wait_recv()
+    received(gathered, 0, 3).wait_recv()
+    normalize(gathered, input_gain, slot)
+    for block in others:
+        pump(0, block)
+    received(gathered, 0, 5).wait_recv()
+    first[6].start()
+    received(gathered, 0, 4).wait_recv()
+    received(gathered, 0, 6).wait_recv()
+    normalize(gathered, input_gain, 1 - slot)
+    for block in others:
+        pump(1, block)
+    ready(5)
+    settle(0)
+    for plane in range(2):
+        rows_out = jnp.dot(
+            normed[plane], joined[...].reshape(width, 4 * group), preferred_element_type=jnp.float32
+        )
+        for i in range(4):
+            projected[i, plane] = (
+                rows_out[:, i * group : (i + 1) * group].astype(jnp.bfloat16).astype(jnp.float32)
+            )
+
+    head_count = rate_ahead.shape[0] // 2
+    head_dim = group // head_count
+    lane = lax.broadcasted_iota(jnp.int32, (length, group), 1)
+    in_lower = lax.rem(lane, head_dim) < head_dim // 2
+
+    def turned(values):
+        partner = jnp.where(
+            in_lower,
+            pltpu.roll(values, group - head_dim // 2, 1),
+            pltpu.roll(values, head_dim // 2, 1),
+        )
+        return values * cosine[...] + partner * sine_part[...]
+
+    offset = (
+        lax.broadcasted_iota(jnp.int32, (length, length), 0)
+        - lax.broadcasted_iota(jnp.int32, (length, length), 1)
+    ).astype(jnp.float32)
+    decays = [
+        jnp.exp(
+            jnp.where(
+                offset >= 0,
+                rate_ahead[slot * head_count + h] * offset,
+                -rate_behind[slot * head_count + h] * offset,
+            )
+        )
+        for h in range(head_count)
+    ]
+    here = [(lane >= h * head_dim) & (lane < (h + 1) * head_dim) for h in range(head_count)]
+    for plane in range(2):
+        queries = turned(projected[0, plane])
+        key_heads = (turned(projected[1, plane]) * head_dim ** (-0.5)).astype(jnp.bfloat16)
+        valued = projected[2, plane]
+        result = jnp.zeros((length, group), jnp.float32)
+        for h in range(head_count):
+            scores = lax.dot_general(
+                jnp.where(here[h], queries, 0.0).astype(jnp.bfloat16),
+                key_heads,
+                (((1,), (1,)), ((), ())),
+                preferred_element_type=jnp.float32,
+            )
+            result = result + jnp.dot(
+                (scores * decays[h]).astype(jnp.bfloat16),
+                jnp.where(here[h], valued, 0.0).astype(jnp.bfloat16),
+                preferred_element_type=jnp.float32,
+            )
+        center = jnp.zeros((length, group), jnp.float32)
+        for h in range(head_count):
+            mean = jnp.sum(jnp.where(here[h], result, 0.0), axis=1, keepdims=True) / head_dim
+            center = jnp.where(here[h], mean, center)
+        centered = result - center
+        squared = centered * centered
+        factor = jnp.zeros((length, group), jnp.float32)
+        for h in range(head_count):
+            spread_h = jnp.sum(jnp.where(here[h], squared, 0.0), axis=1, keepdims=True) / head_dim
+            factor = jnp.where(here[h], lax.rsqrt(spread_h + group_eps), factor)
+        gates = projected[3, plane]
+        mixed[plane] = (gates / (1.0 + jnp.exp(-gates)) * (centered * factor)).astype(jnp.bfloat16)
+
+    ready(6)
+    settle(1)
+
+    def fill(rows_in, weight, partial, side):
+        for x in range(row // 2):
+            block = x * 2 + side
+            for plane in range(2):
+                term = jnp.dot(rows_in[plane], weight[block], preferred_element_type=jnp.float32)
+                partial[side, x, plane] = term.astype(jnp.bfloat16)
+
+    steps = reducer(first_partial, first_core, first_row, first_line, 0)
+    fill(mixed, merge, first_partial, 1 - core)
+    steps[0].start()
+    fill(mixed, merge, first_partial, core)
+    add_core(first_partial, first_core, steps)
+    for block in others:
+        pump(2, block)
+    pass_line(first_partial, first_core, first_row, steps)
+    launch(3)
+    total = tokens[...].astype(jnp.float32) + add_row(
+        first_partial, first_core, first_row, steps, 2
+    )
+    steps[3].wait_recv()
+    total = total + first_line[...].astype(jnp.float32)
+    gathered_mid[slot, seat] = total.astype(jnp.bfloat16)
+
+    second = hand_over(gathered_mid.at[slot, seat], gathered_mid, 1)
+    for step in (2, 1, 0):
+        second[step].start()
+    for i in range(pieces):
+        if i == 0:
+            ready(4)
+        for there in others:
+            post(4 + i, there).start()
+    received(gathered_mid, 1, 1).wait_recv()
+    second[3].start()
+    received(gathered_mid, 1, 2).wait_recv()
+    second[5].start()
+    second[4].start()
+    received(gathered_mid, 1, 0).wait_recv()
+    received(gathered_mid, 1, 3).wait_recv()
+    normalize(gathered_mid, middle_gain, slot)
+    for block in others:
+        pump(3, block)
+    received(gathered_mid, 1, 5).wait_recv()
+    second[6].start()
+    received(gathered_mid, 1, 4).wait_recv()
+    received(gathered_mid, 1, 6).wait_recv()
+    normalize(gathered_mid, middle_gain, 1 - slot)
+    ready(7)
+    ready(8)
+    settle(2)
+    settle(3)
+    tile = 256
+
+    @pl.loop(0, 2)
+    def _(plane):
+        for begin in range(0, hidden_half, tile):
+            columns = slice(begin, min(begin + tile, hidden_half))
+            gate_act, up_act = [
+                jnp.dot(
+                    normed[plane],
+                    weight[:, :, columns].reshape(width, -1),
+                    preferred_element_type=jnp.float32,
+                )
+                for weight in (gate, up)
+            ]
+            hidden[plane, :, columns] = (gate_act / (1.0 + jnp.exp(-gate_act)) * up_act).astype(
+                jnp.bfloat16
+            )
+
+    ready(9)
+    ends = [
+        reducer(last_partial.at[i], last_core.at[i], last_row.at[i], last_line.at[i], 1 + i)
+        for i in range(pieces)
+    ]
+
+    def finish(i):
+        span = slice(i * piece_width, (i + 1) * piece_width)
+        total = gathered_mid[slot, seat, :, span].astype(jnp.float32) + add_row(
+            last_partial.at[i], last_core.at[i], last_row.at[i], ends[i], 2
+        )
+        ends[i][3].wait_recv()
+        out[:, span] = (total + last_line[i].astype(jnp.float32)).astype(jnp.bfloat16)
+
+    for i in range(pieces):
+        for block in others:
+            pump(4 + i, block)
+        settle(4 + i)
+        fill(hidden, down.at[i], last_partial.at[i], 1 - core)
+        ends[i][0].start()
+        fill(hidden, down.at[i], last_partial.at[i], core)
+        add_core(last_partial.at[i], last_core.at[i], ends[i])
+        if i:
+            pass_line(last_partial.at[i - 1], last_core.at[i - 1], last_row.at[i - 1], ends[i - 1])
+    pass_line(last_partial.at[pieces - 1], last_core.at[pieces - 1], last_row.at[pieces - 1], ends[pieces - 1])
+    for i in range(pieces):
+        finish(i)
+
+    for copy in first + second + steps:
+        copy.wait_send()
+    for group_steps in ends:
+        for copy in group_steps:
+            copy.wait_send()
+    for k in range(4 + pieces):
+        for there in others:
+            post(k, there).wait_send()
+            across(k, there, half).wait_send()
+
+
+def paired_call(
+    sizes, flat, input_gain, middle_gain, rates, tables, quads, merge_weight, gate_weight, up_weight, down_weight
+):
+    line, row = sizes["fs"], sizes["tp"]
+    bf16 = jnp.bfloat16
+    length, part_width = flat.shape
+    depth, ret_width = quads[0].shape
+    hidden_half, group = gate_weight.shape[1] // 2, ret_width // 2
+    pieces = 2
+    piece_width = down_weight.shape[1] // pieces
+    kinds = 4 + pieces
+    in_vmem = pl.BlockSpec(memory_space=pltpu.VMEM)
+    in_smem = pl.BlockSpec(memory_space=pltpu.SMEM)
+
+    def sums(lead, columns):
+        return [
+            pltpu.VMEM(lead + (2, row // 2, 2, length, columns), bf16),
+            pltpu.VMEM(lead + (row // 2, 2, length, columns), bf16),
+            pltpu.VMEM(lead + (2, length, columns), bf16),
+            pltpu.VMEM(lead + (length, columns), bf16),
+        ]
+
+    dma = pltpu.SemaphoreType.DMA
+    return pl.pallas_call(
+        functools.partial(paired_kernel, sizes),
+        out_shape=jax.ShapeDtypeStruct(flat.shape, bf16),
+        in_specs=[in_vmem] * 3
+        + [in_smem] * 2
+        + [in_vmem] * 2
+        + [pl.BlockSpec(memory_space=pl.ANY)] * 8,
+        out_specs=in_vmem,
+        scratch_shapes=[
+            pltpu.VMEM((2, depth, 4 * group), bf16),
+            pltpu.VMEM(merge_weight.shape, bf16),
+            pltpu.VMEM(gate_weight.shape, bf16),
+            pltpu.VMEM(up_weight.shape, bf16),
+            pltpu.VMEM(down_weight.shape, bf16),
+            pltpu.VMEM((line, depth, 4 * group), bf16),
+            pltpu.VMEM((line, merge_weight.shape[0] // 2, part_width), bf16),
+            pltpu.VMEM((line, depth, hidden_half), bf16),
+            pltpu.VMEM((line, depth, hidden_half), bf16),
+            pltpu.VMEM((pieces, line, hidden_half, piece_width), bf16),
+            pltpu.VMEM((2, row, length, part_width), bf16),
+            pltpu.VMEM((2, row, length, part_width), bf16),
+            pltpu.VMEM((2, length, row * part_width), bf16),
+            pltpu.VMEM((4, 2, length, group), jnp.float32),
+            pltpu.VMEM((2, length, group), bf16),
+            pltpu.VMEM((2, length, hidden_half), bf16),
+        ]
+        + sums((), part_width)
+        + sums((pieces,), piece_width)
+        + [
+            dma((20 + pieces,)),
+            dma((kinds, line)),
+            dma((kinds, line)),
+            dma((kinds, line)),
+            dma((kinds, line)),
+            dma((2, 7)),
+            dma((2, 7)),
+            dma((1 + pieces, 4)),
+            dma((1 + pieces, 4)),
+        ],
+        compiler_params=pltpu.CompilerParams(
+            collective_id=0, has_side_effects=True, vmem_limit_bytes=60 << 20
+        ),
+    )(
+        flat,
+        input_gain[None, :],
+        middle_gain[None, :],
+        *rates,
+        *tables,
+        *quads,
+        merge_weight,
+        gate_weight,
+        up_weight,
+        down_weight,
+    )
+
+
 def on_device(
     sizes,
     tokens,
@@ -447,7 +1006,35 @@
 ):
     seq_count, length, part_width = tokens.shape
     flat = tokens.reshape(seq_count * length, part_width)
-    joined = jnp.concatenate([query_weight, key_weight, value_weight, output_gate_matrix], axis=1)
+    quads = (query_weight, key_weight, value_weight, output_gate_matrix)
+    paired = (
+        sizes["grp"] == 2
+        and sizes["fs"] == sizes["tp"] == 4
+        and seq_count == 1
+        and query_weight.shape[1] % 256 == 0
+        and forward_decay.shape[0] % 2 == 0
+        and gate_weight.shape[1] % 256 == 0
+        and down_weight.shape[1] == part_width
+        and part_width % 256 == 0
+    )
+    if paired:
+        head_count = forward_decay.shape[0] // 2
+        head_dim = query_weight.shape[1] // (2 * head_count)
+        layer_out = paired_call(
+            sizes,
+            flat,
+            input_gain,
+            middle_gain,
+            (jax.nn.log_sigmoid(forward_decay), jax.nn.log_sigmoid(backward_decay)),
+            turn_tables(length, head_dim, head_count),
+            quads,
+            merge_weight,
+            gate_weight,
+            up_weight,
+            down_weight,
+        )
+        return layer_out.reshape(seq_count, length, part_width)
+    joined = jnp.concatenate(quads, axis=1)
     shards = (joined, merge_weight, gate_weight, up_weight, down_weight)
     line, copies, row = sizes["fs"], sizes["grp"], sizes["tp"]
     down_width = down_weight.shape[1]

time: 220 us -> 184 us (0.84)
  Pallas kernels: 213 us -> 181 us
  other arithmetic: 3.59 us -> 1.22 us
    pallas_call x1, Pallas kernels: 213 us -> 181 us  [paired_call(): pl.pallas_call(functools.partial(paired_kernel, sizes), out_shape=jax.Sha...]
    concatenate x1 -> x0, other arithmetic: 2.32 us -> none  [on_device(): jnp.concatenate([query_weight, key_weight, value_weight, output_gate_matr...]
where the time goes in v1:
time: 184 us
  Pallas kernels  181 us (98%)
    pallas_call x1, Pallas kernels, paired_call(): pl.pallas_call(functools.partial(paired_kernel, sizes), out_shape=jax.Sha...  181 us

profile of v1, /device:TPU:0, one launch (start us, length us, event | category | flops | bytes accessed | tf_op | source)
XLA Modules:
  0.0 183.8 jit_solution(3144669308340634983)
XLA Ops:
  0.0 1.2 fusion
  1.2 180.8 %shard_map.145 = bf16[384,512]{1,0:T(8,128)(2,1)} custom-call(bf16[384,512]{1,0:T(8,128)(2,1)} %bitcast.5, f32[1,2048]{1,0:T(1,128)} %bitcast.6, f32[1,2048]{1,0:T(1,128)} %bitcast.7, f32[4]{0:T(128)} %get-tuple-element.5.rate_ahead, f32[4]{0:T(128)} %get-tuple-element.6.rate_behind, f32[384,128]{1,0:T(8,128)} %constant.9.clone.cosine, ...), custom_call_target="tpu_custom_call" | custom-call | tf_op jit(solution)/shard_map/pallas_call | solution.py:935
  182.0 1.8 copy.17

commit v2 on v1

--- a/solution.py
+++ b/solution.py
@@ -676,36 +676,59 @@
             device_id_type=MESH,
         )
 
-    def reducer(partial, core_in, row_in, line_in, stage):
-        return [
-            moved(partial.at[1 - core], core_in, {"tp": core_peer}, stage, 0),
-            moved(partial.at[core, 1 - column, 1 - slot], row_in.at[0], {"tp": row_peer}, stage, 1),
-            moved(partial.at[core, 1 - column, slot], row_in.at[1], {"tp": row_peer}, stage, 2),
-            moved(partial.at[core, column, 1 - slot], line_in, {"fs": line_peer}, stage, 3),
+    def share_mid(step):
+        plane, kind = step % 2, step // 2
+        spot = gathered_mid.at[plane, row_peer if kind == 2 else seat]
+        return pltpu.make_async_remote_copy(
+            src_ref=spot,
+            dst_ref=spot,
+            send_sem=share_send.at[1, step],
+            recv_sem=share_recv.at[1, step],
+            device_id={"tp": core_peer if kind else row_peer},
+            device_id_type=MESH,
+        )
+
+    def shared_mid(step):
+        plane, kind = step % 2, step // 2
+        spot = gathered_mid.at[plane, (row_peer, core_peer, far_peer)[kind]]
+        return pltpu.make_async_remote_copy(
+            src_ref=spot,
+            dst_ref=spot,
+            send_sem=share_send.at[1, step],
+            recv_sem=share_recv.at[1, step],
+            device_id={"tp": core_peer},
+            device_id_type=MESH,
+        )
+
+    def reducer(partial, core_in, row_in, stage):
+        order = (0, 1) if stage == 0 else (1 - slot, slot)
+        return [moved(partial.at[1 - core], core_in, {"tp": core_peer}, stage, 0)] + [
+            moved(
+                partial.at[core, 1 - column, plane],
+                row_in.at[step],
+                {"tp": row_peer},
+                stage,
+                1 + step,
+            )
+            for step, plane in enumerate(order)
         ]
 
-    def add_core(partial, core_in, steps):
+    def add_core(partial, core_in, steps, order):
         steps[0].wait_recv()
-        for step, plane in ((1, 1 - slot), (2, slot)):
+        for step, plane in enumerate(order):
             total = partial[core, 1 - column, plane].astype(jnp.float32) + core_in[
                 1 - column, plane
             ].astype(jnp.float32)
             partial[core, 1 - column, plane] = total.astype(jnp.bfloat16)
-            steps[step].start()
-
-    def add_row(partial, core_in, row_in, steps, step):
-        plane = 1 - slot if step == 1 else slot
-        steps[step].wait_recv()
+            steps[1 + step].start()
+
+    def add_row(partial, core_in, row_in, steps, step, plane):
+        steps[1 + step].wait_recv()
         return (
             partial[core, column, plane].astype(jnp.float32)
             + core_in[column, plane].astype(jnp.float32)
-            + row_in[step - 1].astype(jnp.float32)
-        )
-
-    def pass_line(partial, core_in, row_in, steps):
-        total = add_row(partial, core_in, row_in, steps, 1)
-        partial[core, column, 1 - slot] = total.astype(jnp.bfloat16)
-        steps[3].start()
+            + row_in[step].astype(jnp.float32)
+        )
 
     first = hand_over(tokens, gathered, 0)
     for step in (2, 1, 0):
@@ -809,53 +832,53 @@
                 term = jnp.dot(rows_in[plane], weight[block], preferred_element_type=jnp.float32)
                 partial[side, x, plane] = term.astype(jnp.bfloat16)
 
-    steps = reducer(first_partial, first_core, first_row, first_line, 0)
+    steps = reducer(first_partial, first_core, first_row, 0) + [
+        moved(first_partial.at[core, column, plane], first_line.at[plane], {"fs": line_peer}, 0, 3 + plane)
+        for plane in range(2)
+    ]
     fill(mixed, merge, first_partial, 1 - core)
     steps[0].start()
+    pump(2, others[0])
     fill(mixed, merge, first_partial, core)
-    add_core(first_partial, first_core, steps)
-    for block in others:
-        pump(2, block)
-    pass_line(first_partial, first_core, first_row, steps)
+    pump(2, others[1])
+    add_core(first_partial, first_core, steps, (0, 1))
+    pump(2, others[2])
+    for plane in range(2):
+        total = add_row(first_partial, first_core, first_row, steps, plane, plane)
+        first_partial[core, column, plane] = total.astype(jnp.bfloat16)
+        steps[3 + plane].start()
     launch(3)
-    total = tokens[...].astype(jnp.float32) + add_row(
-        first_partial, first_core, first_row, steps, 2
-    )
-    steps[3].wait_recv()
-    total = total + first_line[...].astype(jnp.float32)
-    gathered_mid[slot, seat] = total.astype(jnp.bfloat16)
-
-    second = hand_over(gathered_mid.at[slot, seat], gathered_mid, 1)
-    for step in (2, 1, 0):
-        second[step].start()
+    ready(4)
     for i in range(pieces):
-        if i == 0:
-            ready(4)
         for there in others:
             post(4 + i, there).start()
-    received(gathered_mid, 1, 1).wait_recv()
-    second[3].start()
-    received(gathered_mid, 1, 2).wait_recv()
-    second[5].start()
-    second[4].start()
-    received(gathered_mid, 1, 0).wait_recv()
-    received(gathered_mid, 1, 3).wait_recv()
-    normalize(gathered_mid, middle_gain, slot)
-    for block in others:
-        pump(3, block)
-    received(gathered_mid, 1, 5).wait_recv()
-    second[6].start()
-    received(gathered_mid, 1, 4).wait_recv()
-    received(gathered_mid, 1, 6).wait_recv()
-    normalize(gathered_mid, middle_gain, 1 - slot)
+
+    second = [share_mid(step) for step in range(6)]
+    for plane in range(2):
+        steps[3 + plane].wait_recv()
+        total = gathered[plane, seat].astype(jnp.float32) + (
+            first_partial[core, column, plane].astype(jnp.float32)
+            + first_line[plane].astype(jnp.float32)
+        )
+        gathered_mid[plane, seat] = total.astype(jnp.bfloat16)
+        second[plane].start()
+        second[2 + plane].start()
+    for plane in range(2):
+        pump(3, others[plane])
+        shared_mid(plane).wait_recv()
+        second[4 + plane].start()
+    pump(3, others[2])
+    for plane in range(2):
+        shared_mid(2 + plane).wait_recv()
+        shared_mid(4 + plane).wait_recv()
+        normalize(gathered_mid, middle_gain, plane)
+        pump(4, others[plane])
     ready(7)
     ready(8)
     settle(2)
     settle(3)
     tile = 256
-
-    @pl.loop(0, 2)
-    def _(plane):
+    for plane in range(2):
         for begin in range(0, hidden_half, tile):
             columns = slice(begin, min(begin + tile, hidden_half))
             gate_act, up_act = [
@@ -869,32 +892,50 @@
             hidden[plane, :, columns] = (gate_act / (1.0 + jnp.exp(-gate_act)) * up_act).astype(
                 jnp.bfloat16
             )
+        pump(4 + plane, others[2 * (1 - plane)])
 
     ready(9)
     ends = [
-        reducer(last_partial.at[i], last_core.at[i], last_row.at[i], last_line.at[i], 1 + i)
+        reducer(last_partial.at[i], last_core.at[i], last_row.at[i], 1 + i)
+        + [
+            moved(
+                last_partial.at[i, core, column, 1 - slot],
+                last_line.at[i],
+                {"fs": line_peer},
+                1 + i,
+                3,
+            )
+        ]
         for i in range(pieces)
     ]
+
+    def pass_line(i):
+        total = add_row(
+            last_partial.at[i], last_core.at[i], last_row.at[i], ends[i], 0, 1 - slot
+        )
+        last_partial[i, core, column, 1 - slot] = total.astype(jnp.bfloat16)
+        ends[i][3].start()
 
     def finish(i):
         span = slice(i * piece_width, (i + 1) * piece_width)
         total = gathered_mid[slot, seat, :, span].astype(jnp.float32) + add_row(
-            last_partial.at[i], last_core.at[i], last_row.at[i], ends[i], 2
+            last_partial.at[i], last_core.at[i], last_row.at[i], ends[i], 1, slot
         )
         ends[i][3].wait_recv()
         out[:, span] = (total + last_line[i].astype(jnp.float32)).astype(jnp.bfloat16)
 
     for i in range(pieces):
-        for block in others:
-            pump(4 + i, block)
+        if i:
+            for block in others[1:] if i == 1 else others:
+                pump(4 + i, block)
         settle(4 + i)
         fill(hidden, down.at[i], last_partial.at[i], 1 - core)
         ends[i][0].start()
         fill(hidden, down.at[i], last_partial.at[i], core)
-        add_core(last_partial.at[i], last_core.at[i], ends[i])
+        add_core(last_partial.at[i], last_core.at[i], ends[i], (1 - slot, slot))
         if i:
-            pass_line(last_partial.at[i - 1], last_core.at[i - 1], last_row.at[i - 1], ends[i - 1])
-    pass_line(last_partial.at[pieces - 1], last_core.at[pieces - 1], last_row.at[pieces - 1], ends[pieces - 1])
+            pass_line(i - 1)
+    pass_line(pieces - 1)
     for i in range(pieces):
         finish(i)
 
@@ -923,12 +964,12 @@
     in_vmem = pl.BlockSpec(memory_space=pltpu.VMEM)
     in_smem = pl.BlockSpec(memory_space=pltpu.SMEM)
 
-    def sums(lead, columns):
+    def sums(lead, columns, last):
         return [
             pltpu.VMEM(lead + (2, row // 2, 2, length, columns), bf16),
             pltpu.VMEM(lead + (row // 2, 2, length, columns), bf16),
             pltpu.VMEM(lead + (2, length, columns), bf16),
-            pltpu.VMEM(lead + (length, columns), bf16),
+            pltpu.VMEM(lead + last + (length, columns), bf16),
         ]
 
     dma = pltpu.SemaphoreType.DMA
@@ -958,8 +999,8 @@
             pltpu.VMEM((2, length, group), bf16),
             pltpu.VMEM((2, length, hidden_half), bf16),
         ]
-        + sums((), part_width)
-        + sums((pieces,), piece_width)
+        + sums((), part_width, (2,))
+        + sums((pieces,), piece_width, ())
         + [
             dma((20 + pieces,)),
             dma((kinds, line)),
@@ -968,8 +1009,8 @@
             dma((kinds, line)),
             dma((2, 7)),
             dma((2, 7)),
-            dma((1 + pieces, 4)),
-            dma((1 + pieces, 4)),
+            dma((1 + pieces, 5)),
+            dma((1 + pieces, 5)),
         ],
         compiler_params=pltpu.CompilerParams(
             collective_id=0, has_side_effects=True, vmem_limit_bytes=60 << 20

time: 184 us -> 164 us (0.89)
  Pallas kernels: 181 us -> 161 us
    pallas_call x1, Pallas kernels: 181 us -> 161 us  [paired_call(): pl.pallas_call(functools.partial(paired_kernel, sizes), out_shape=jax.Sha...]
where the time goes in v2:
time: 164 us
  Pallas kernels  161 us (98%)
  local copies, waits for them, and re-layouts  1.77 us (1%)
    pallas_call x1, Pallas kernels, paired_call(): pl.pallas_call(functools.partial(paired_kernel, sizes), out_shape=jax.Sha...  161 us

profile of v2, /device:TPU:0, one launch (start us, length us, event | category | flops | bytes accessed | tf_op | source)
XLA Modules:
  0.0 164.3 jit_solution(5526913925761336833)
XLA Ops:
  0.0 1.2 fusion
  1.2 161.3 %shard_map.145 = bf16[384,512]{1,0:T(8,128)(2,1)} custom-call(bf16[384,512]{1,0:T(8,128)(2,1)} %bitcast.5, f32[1,2048]{1,0:T(1,128)} %bitcast.6, f32[1,2048]{1,0:T(1,128)} %bitcast.7, f32[4]{0:T(128)} %get-tuple-element.5.rate_ahead, f32[4]{0:T(128)} %get-tuple-element.6.rate_behind, f32[384,128]{1,0:T(8,128)} %constant.9.clone.cosine, ...), custom_call_target="tpu_custom_call" | custom-call | tf_op jit(solution)/shard_map/pallas_call | solution.py:976
  162.5 1.8 %copy.17 = bf16[1,384,512]{2,1,0:T(8,128)(2,1)} copy(bf16[1,384,512]{2,1,0:T(8,128)(2,1)} %bitcast.4) | data formatting | bytes 786432

commit v3 on v2

--- a/solution.py
+++ b/solution.py
@@ -736,6 +736,7 @@
     launch(0)
     launch(1)
     launch(2)
+    launch(3)
     received(gathered, 0, 1).wait_recv()
     first[3].start()
     received(gathered, 0, 2).wait_recv()
@@ -838,22 +839,21 @@
     ]
     fill(mixed, merge, first_partial, 1 - core)
     steps[0].start()
-    pump(2, others[0])
     fill(mixed, merge, first_partial, core)
-    pump(2, others[1])
     add_core(first_partial, first_core, steps, (0, 1))
-    pump(2, others[2])
+    for block in others:
+        pump(2, block)
     for plane in range(2):
         total = add_row(first_partial, first_core, first_row, steps, plane, plane)
         first_partial[core, column, plane] = total.astype(jnp.bfloat16)
         steps[3 + plane].start()
-    launch(3)
     ready(4)
     for i in range(pieces):
         for there in others:
             post(4 + i, there).start()
 
     second = [share_mid(step) for step in range(6)]
+    pump(3, others[0])
     for plane in range(2):
         steps[3 + plane].wait_recv()
         total = gathered[plane, seat].astype(jnp.float32) + (
@@ -863,16 +863,21 @@
         gathered_mid[plane, seat] = total.astype(jnp.bfloat16)
         second[plane].start()
         second[2 + plane].start()
+        pump(3, others[1 + plane])
+    queue = [(4 + i, block) for i in range(pieces) for block in others]
+
+    def pump_next(count):
+        for _ in range(count):
+            pump(*queue.pop(0))
+
     for plane in range(2):
-        pump(3, others[plane])
         shared_mid(plane).wait_recv()
         second[4 + plane].start()
-    pump(3, others[2])
     for plane in range(2):
         shared_mid(2 + plane).wait_recv()
         shared_mid(4 + plane).wait_recv()
         normalize(gathered_mid, middle_gain, plane)
-        pump(4, others[plane])
+    pump_next(len(others))
     ready(7)
     ready(8)
     settle(2)
@@ -892,7 +897,7 @@
             hidden[plane, :, columns] = (gate_act / (1.0 + jnp.exp(-gate_act)) * up_act).astype(
                 jnp.bfloat16
             )
-        pump(4 + plane, others[2 * (1 - plane)])
+    pump_next(len(others))
 
     ready(9)
     ends = [
@@ -925,9 +930,8 @@
         out[:, span] = (total + last_line[i].astype(jnp.float32)).astype(jnp.bfloat16)
 
     for i in range(pieces):
-        if i:
-            for block in others[1:] if i == 1 else others:
-                pump(4 + i, block)
+        if i + 1 < pieces and queue and queue[0][0] == 5 + i:
+            pump_next(len(others))
         settle(4 + i)
         fill(hidden, down.at[i], last_partial.at[i], 1 - core)
         ends[i][0].start()
@@ -958,7 +962,7 @@
     length, part_width = flat.shape
     depth, ret_width = quads[0].shape
     hidden_half, group = gate_weight.shape[1] // 2, ret_width // 2
-    pieces = 2
+    pieces = 4
     piece_width = down_weight.shape[1] // pieces
     kinds = 4 + pieces
     in_vmem = pl.BlockSpec(memory_space=pltpu.VMEM)

time: 164 us -> 148 us (0.902)
  Pallas kernels: 161 us -> 145 us
    pallas_call x1, Pallas kernels: 161 us -> 145 us  [paired_call(): pl.pallas_call(functools.partial(paired_kernel, sizes), out_shape=jax.Sha...]
where the time goes in v3:
time: 148 us
  Pallas kernels  145 us (98%)
  local copies, waits for them, and re-layouts  1.77 us (1%)
    pallas_call x1, Pallas kernels, paired_call(): pl.pallas_call(functools.partial(paired_kernel, sizes), out_shape=jax.Sha...  145 us

profile of v3, /device:TPU:0, one launch (start us, length us, event | category | flops | bytes accessed | tf_op | source)
XLA Modules:
  0.0 147.7 jit_solution(2516625849187270837)
XLA Ops:
  0.0 1.2 fusion
  1.2 144.7 %shard_map.145 = bf16[384,512]{1,0:T(8,128)(2,1)} custom-call(bf16[384,512]{1,0:T(8,128)(2,1)} %bitcast.5, f32[1,2048]{1,0:T(1,128)} %bitcast.6, f32[1,2048]{1,0:T(1,128)} %bitcast.7, f32[4]{0:T(128)} %get-tuple-element.5.rate_ahead, f32[4]{0:T(128)} %get-tuple-element.6.rate_behind, f32[384,128]{1,0:T(8,128)} %constant.9.clone.cosine, ...), custom_call_target="tpu_custom_call" | custom-call | tf_op jit(solution)/shard_map/pallas_call | solution.py:980
  145.9 1.8 %copy.17 = bf16[1,384,512]{2,1,0:T(8,128)(2,1)} copy(bf16[1,384,512]{2,1,0:T(8,128)(2,1)} %bitcast.4) | data formatting | bytes 786432

commit v4 on v3

--- a/solution.py
+++ b/solution.py
@@ -432,12 +432,12 @@
 def paired_kernel(
     sizes,
     tokens,
-    input_gain,
-    middle_gain,
-    rate_ahead,
-    rate_behind,
-    cosine,
-    sine_part,
+    input_gain_in,
+    middle_gain_in,
+    ahead,
+    behind,
+    cosine_in,
+    sine_in,
     query_shard,
     key_shard,
     value_shard,
@@ -447,6 +447,11 @@
     up_shard,
     down_shard,
     out,
+    input_gain,
+    middle_gain,
+    cosine,
+    sine_part,
+    finished,
     joined_out,
     merge_out,
     gate_out,
@@ -480,6 +485,7 @@
     share_recv,
     sum_send,
     sum_recv,
+    out_sem,
 ):
     line, row = sizes["fs"], sizes["tp"]
     pieces = down.shape[0]
@@ -497,6 +503,10 @@
     line_peer = place + 1 - 2 * slot
     sign = 1 - 2 * (place // (line // 2))
     others = [lax.rem(place + sign * step + line, line) for step in range(1, line)]
+    facing = jnp.where(place < line // 2, line // 2, line // 2 - 1)
+    sources = [facing, line_peer] + [
+        facing + sign * step for step in range(1, line // 2)
+    ]
 
     barrier = pltpu.get_barrier_semaphore()
     for there in others:
@@ -538,6 +548,13 @@
             )
             for i in range(pieces)
         ],
+        [(tokens, gathered.at[slot, seat])],
+        [
+            (input_gain_in, input_gain),
+            (middle_gain_in, middle_gain),
+            (cosine_in, cosine),
+            (sine_in, sine_part),
+        ],
     ]
     own, index = [], 0
     for pairs in loads:
@@ -545,10 +562,9 @@
         for source, target in pairs:
             own[-1].append(pltpu.make_async_copy(source, target, own_sem.at[index]))
             index += 1
-    for copies in own:
+    for copies in (own[-2], *own[:-2], own[-1]):
         for copy in copies:
             copy.start()
-    gathered[slot, seat] = tokens[...]
     pl.semaphore_wait(barrier, line - 1 + 1 + 2)
 
     def ready(k):
@@ -618,10 +634,10 @@
         across(k, block, half).start()
 
     def settle(k):
-        for block in others:
+        for block in sources:
             across(k, block, 1 - half).wait_recv()
 
-    def handed(source, target, stage, step):
+    def handed(target, stage, step):
         plane = slot if step in (0, 1, 2, 3) else 1 - slot
         holder = seat if step in (0, 1, 2, 4, 5) else row_peer
         place_in = target.at[plane, holder]
@@ -631,7 +647,7 @@
         if step == 2:
             peer = {"fs": line_peer}
         return pltpu.make_async_remote_copy(
-            src_ref=source if step < 3 else place_in,
+            src_ref=place_in,
             dst_ref=place_in,
             send_sem=share_send.at[stage, step],
             recv_sem=share_recv.at[stage, step],
@@ -663,8 +679,8 @@
             scaled = source[plane, t].astype(jnp.float32) * scale * gain_vector[:, span]
             normed[plane, :, span] = scaled.astype(jnp.bfloat16)
 
-    def hand_over(source, target, stage):
-        return [handed(source, target, stage, step) for step in range(7)]
+    def hand_over(target, stage):
+        return [handed(target, stage, step) for step in range(7)]
 
     def moved(source, target, peer, stage, step):
         return pltpu.make_async_remote_copy(
@@ -730,7 +746,8 @@
             + row_in[step].astype(jnp.float32)
         )
 
-    first = hand_over(tokens, gathered, 0)
+    first = hand_over(gathered, 0)
+    ready(10)
     for step in (2, 1, 0):
         first[step].start()
     launch(0)
@@ -739,23 +756,25 @@
     launch(3)
     received(gathered, 0, 1).wait_recv()
     first[3].start()
+    pump(0, sources[0])
     received(gathered, 0, 2).wait_recv()
     first[5].start()
     first[4].start()
+    pump(0, sources[1])
     received(gathered, 0, 0).wait_recv()
     received(gathered, 0, 3).wait_recv()
+    ready(11)
     normalize(gathered, input_gain, slot)
-    for block in others:
-        pump(0, block)
+    pump(0, sources[2])
     received(gathered, 0, 5).wait_recv()
     first[6].start()
     received(gathered, 0, 4).wait_recv()
     received(gathered, 0, 6).wait_recv()
     normalize(gathered, input_gain, 1 - slot)
-    for block in others:
-        pump(1, block)
     ready(5)
     settle(0)
+    for block in sources:
+        pump(1, block)
     for plane in range(2):
         rows_out = jnp.dot(
             normed[plane], joined[...].reshape(width, 4 * group), preferred_element_type=jnp.float32
@@ -765,7 +784,7 @@
                 rows_out[:, i * group : (i + 1) * group].astype(jnp.bfloat16).astype(jnp.float32)
             )
 
-    head_count = rate_ahead.shape[0] // 2
+    head_count = ahead.shape[0] // 2
     head_dim = group // head_count
     lane = lax.broadcasted_iota(jnp.int32, (length, group), 1)
     in_lower = lax.rem(lane, head_dim) < head_dim // 2
@@ -782,12 +801,17 @@
         lax.broadcasted_iota(jnp.int32, (length, length), 0)
         - lax.broadcasted_iota(jnp.int32, (length, length), 1)
     ).astype(jnp.float32)
+
+    def log_sigmoid(logit):
+        value = jnp.full((8, 128), logit, jnp.float32)
+        return (jnp.minimum(value, 0.0) - jnp.log1p(jnp.exp(-jnp.abs(value))))[:1, :1]
+
     decays = [
         jnp.exp(
             jnp.where(
                 offset >= 0,
-                rate_ahead[slot * head_count + h] * offset,
-                -rate_behind[slot * head_count + h] * offset,
+                log_sigmoid(ahead[slot * head_count + h]) * offset,
+                -log_sigmoid(behind[slot * head_count + h]) * offset,
             )
         )
         for h in range(head_count)
@@ -841,8 +865,7 @@
     steps[0].start()
     fill(mixed, merge, first_partial, core)
     add_core(first_partial, first_core, steps, (0, 1))
-    for block in others:
-        pump(2, block)
+    pump(2, others[0])
     for plane in range(2):
         total = add_row(first_partial, first_core, first_row, steps, plane, plane)
         first_partial[core, column, plane] = total.astype(jnp.bfloat16)
@@ -853,6 +876,8 @@
             post(4 + i, there).start()
 
     second = [share_mid(step) for step in range(6)]
+    pump(2, others[1])
+    pump(2, others[2])
     pump(3, others[0])
     for plane in range(2):
         steps[3 + plane].wait_recv()
@@ -873,11 +898,11 @@
     for plane in range(2):
         shared_mid(plane).wait_recv()
         second[4 + plane].start()
+        pump_next(len(others))
     for plane in range(2):
         shared_mid(2 + plane).wait_recv()
         shared_mid(4 + plane).wait_recv()
         normalize(gathered_mid, middle_gain, plane)
-    pump_next(len(others))
     ready(7)
     ready(8)
     settle(2)
@@ -897,7 +922,8 @@
             hidden[plane, :, columns] = (gate_act / (1.0 + jnp.exp(-gate_act)) * up_act).astype(
                 jnp.bfloat16
             )
-    pump_next(len(others))
+        if plane == 0:
+            pump_next(len(others))
 
     ready(9)
     ends = [
@@ -921,17 +947,27 @@
         last_partial[i, core, column, 1 - slot] = total.astype(jnp.bfloat16)
         ends[i][3].start()
 
+    written = [
+        pltpu.make_async_copy(
+            finished.at[:, i * piece_width : (i + 1) * piece_width],
+            out.at[:, i * piece_width : (i + 1) * piece_width],
+            out_sem.at[i],
+        )
+        for i in range(pieces)
+    ]
+
     def finish(i):
         span = slice(i * piece_width, (i + 1) * piece_width)
         total = gathered_mid[slot, seat, :, span].astype(jnp.float32) + add_row(
             last_partial.at[i], last_core.at[i], last_row.at[i], ends[i], 1, slot
         )
         ends[i][3].wait_recv()
-        out[:, span] = (total + last_line[i].astype(jnp.float32)).astype(jnp.bfloat16)
+        finished[:, span] = (total + last_line[i].astype(jnp.float32)).astype(jnp.bfloat16)
+        written[i].start()
 
     for i in range(pieces):
-        if i + 1 < pieces and queue and queue[0][0] == 5 + i:
-            pump_next(len(others))
+        if i == 2:
+            pump_next(len(queue))
         settle(4 + i)
         fill(hidden, down.at[i], last_partial.at[i], 1 - core)
         ends[i][0].start()
@@ -939,10 +975,14 @@
         add_core(last_partial.at[i], last_core.at[i], ends[i], (1 - slot, slot))
         if i:
             pass_line(i - 1)
+        if i > 1:
+            finish(i - 2)
     pass_line(pieces - 1)
-    for i in range(pieces):
+    for i in range(max(0, pieces - 2), pieces):
         finish(i)
 
+    for copy in written:
+        copy.wait()
     for copy in first + second + steps:
         copy.wait_send()
     for group_steps in ends:
@@ -955,7 +995,7 @@
 
 
 def paired_call(
-    sizes, flat, input_gain, middle_gain, rates, tables, quads, merge_weight, gate_weight, up_weight, down_weight
+    sizes, flat, input_gain, middle_gain, decays, tables, quads, merge_weight, gate_weight, up_weight, down_weight
 ):
     line, row = sizes["fs"], sizes["tp"]
     bf16 = jnp.bfloat16
@@ -965,7 +1005,7 @@
     pieces = 4
     piece_width = down_weight.shape[1] // pieces
     kinds = 4 + pieces
-    in_vmem = pl.BlockSpec(memory_space=pltpu.VMEM)
+    anywhere = pl.BlockSpec(memory_space=pl.ANY)
     in_smem = pl.BlockSpec(memory_space=pltpu.SMEM)
 
     def sums(lead, columns, last):
@@ -980,12 +1020,14 @@
     return pl.pallas_call(
         functools.partial(paired_kernel, sizes),
         out_shape=jax.ShapeDtypeStruct(flat.shape, bf16),
-        in_specs=[in_vmem] * 3
-        + [in_smem] * 2
-        + [in_vmem] * 2
-        + [pl.BlockSpec(memory_space=pl.ANY)] * 8,
-        out_specs=in_vmem,
+        in_specs=[anywhere] * 3 + [in_smem] * 2 + [anywhere] * 10,
+        out_specs=anywhere,
         scratch_shapes=[
+            pltpu.VMEM((1, row * part_width), jnp.float32),
+            pltpu.VMEM((1, row * part_width), jnp.float32),
+            pltpu.VMEM(tables[0].shape, jnp.float32),
+            pltpu.VMEM(tables[1].shape, jnp.float32),
+            pltpu.VMEM(flat.shape, bf16),
             pltpu.VMEM((2, depth, 4 * group), bf16),
             pltpu.VMEM(merge_weight.shape, bf16),
             pltpu.VMEM(gate_weight.shape, bf16),
@@ -1006,7 +1048,7 @@
         + sums((), part_width, (2,))
         + sums((pieces,), piece_width, ())
         + [
-            dma((20 + pieces,)),
+            dma((25 + pieces,)),
             dma((kinds, line)),
             dma((kinds, line)),
             dma((kinds, line)),
@@ -1015,6 +1057,7 @@
             dma((2, 7)),
             dma((1 + pieces, 5)),
             dma((1 + pieces, 5)),
+            dma((pieces,)),
         ],
         compiler_params=pltpu.CompilerParams(
             collective_id=0, has_side_effects=True, vmem_limit_bytes=60 << 20
@@ -1023,7 +1066,7 @@
         flat,
         input_gain[None, :],
         middle_gain[None, :],
-        *rates,
+        *decays,
         *tables,
         *quads,
         merge_weight,
@@ -1070,7 +1113,7 @@
             flat,
             input_gain,
             middle_gain,
-            (jax.nn.log_sigmoid(forward_decay), jax.nn.log_sigmoid(backward_decay)),
+            (forward_decay, backward_decay),
             turn_tables(length, head_dim, head_count),
             quads,
             merge_weight,

time: 148 us -> 144 us (0.973)
  Pallas kernels: 145 us -> 142 us
    pallas_call x1, Pallas kernels: 145 us -> 142 us  [paired_call(): pl.pallas_call(functools.partial(paired_kernel, sizes), out_shape=jax.Sha...]
where the time goes in v4:
time: 144 us
  Pallas kernels  142 us (99%)
  local copies, waits for them, and re-layouts  1.77 us (1%)
    pallas_call x1, Pallas kernels, paired_call(): pl.pallas_call(functools.partial(paired_kernel, sizes), out_shape=jax.Sha...  142 us

profile of v4, /device:TPU:0, one launch (start us, length us, event | category | flops | bytes accessed | tf_op | source)
XLA Modules:
  0.0 144.0 jit_solution(1695812980883510593)
XLA Ops:
  0.0 142.2 %shard_map.145 = bf16[384,512]{1,0:T(8,128)(2,1)} custom-call(bf16[384,512]{1,0:T(8,128)(2,1)} %bitcast.5, f32[1,2048]{1,0:T(1,128)} %bitcast.6, f32[1,2048]{1,0:T(1,128)} %bitcast.7, f32[4]{0:T(128)} %ahead.1, f32[4]{0:T(128)} %behind.1, f32[384,128]{1,0:T(8,128)} %constant.4.clone.cosine_in, f32[384,128]{1,0:T(8,128)} %constant.5.clone.sine_in, ...), custom_call_target="tpu_custom_call" | custom-call | tf_op jit(solution)/shard_map/pallas_call | solution.py:1020
  142.2 1.8 %copy.17 = bf16[1,384,512]{2,1,0:T(8,128)(2,1)} copy(bf16[1,384,512]{2,1,0:T(8,128)(2,1)} %bitcast.4) | data formatting | bytes 786432

commit v5 on v4

--- a/solution.py
+++ b/solution.py
@@ -504,9 +504,8 @@
     sign = 1 - 2 * (place // (line // 2))
     others = [lax.rem(place + sign * step + line, line) for step in range(1, line)]
     facing = jnp.where(place < line // 2, line // 2, line // 2 - 1)
-    sources = [facing, line_peer] + [
-        facing + sign * step for step in range(1, line // 2)
-    ]
+    crossing = [facing + sign * step for step in range(line // 2)]
+    sources = [facing, line_peer] + crossing[1:]
 
     barrier = pltpu.get_barrier_semaphore()
     for there in others:
@@ -562,14 +561,18 @@
         for source, target in pairs:
             own[-1].append(pltpu.make_async_copy(source, target, own_sem.at[index]))
             index += 1
+
     for copies in (own[-2], *own[:-2], own[-1]):
         for copy in copies:
             copy.start()
+
     pl.semaphore_wait(barrier, line - 1 + 1 + 2)
 
     def ready(k):
         for copy in own[k]:
             copy.wait()
+
+    first_down = 6
 
     def outgoing(k, parity):
         if k == 0:
@@ -578,20 +581,23 @@
         if k == 1:
             size = merge_rows // 2
             return cut(merge_out, 0, parity * 2 + half, size)
-        if k < 4:
-            source = (gate_out, up_out)[k - 2]
-            size = source.shape[0] // 2
-            return cut(source, 0, half, size).at[
+        if k < first_down:
+            source = (gate_out, up_out)[(k - 2) // 2]
+            size = source.shape[0] // 4
+            return cut(source, 0, half * 2 + k % 2, size).at[
                 :, pl.ds(pl.multiple_of(parity * hidden_half, hidden_half), hidden_half)
             ]
         size = hidden_half // 2
-        return cut(down_out, 0, parity * 2 + half, size).at[
-            :, (k - 4) * piece_width : (k - 3) * piece_width
-        ]
+        begin = (k - first_down) * piece_width
+        return cut(down_out, 0, parity * 2 + half, size).at[:, begin : begin + piece_width]
 
     def landing(k, block, part):
-        target = (joined, merge, gate, up)[k] if k < 4 else down.at[k - 4]
-        size = target.shape[1] // 2
+        if 2 <= k < first_down:
+            target = (gate, up)[(k - 2) // 2]
+            size, part = target.shape[1] // 4, part * 2 + k % 2
+        else:
+            target = (joined, merge)[k] if k < 2 else down.at[k - first_down]
+            size = target.shape[1] // 2
         return target.at[block, pl.ds(pl.multiple_of(part * size, size), size)]
 
     def post(k, there):
@@ -625,7 +631,6 @@
         )
 
     def launch(k):
-        ready(k)
         for there in others:
             post(k, there).start()
 
@@ -716,65 +721,86 @@
             device_id_type=MESH,
         )
 
-    def reducer(partial, core_in, row_in, stage):
-        order = (0, 1) if stage == 0 else (1 - slot, slot)
+    def spot(by_row, ahead_part, behind_part):
+        return (ahead_part, behind_part) if by_row else (behind_part, ahead_part)
+
+    def chosen(by_row):
+        return spot(by_row, column, slot)
+
+    def reducer(partial, core_in, row_in, stage, order, by_row):
+        mine = chosen(by_row)[0]
+        peer = {"tp": row_peer} if by_row else {"fs": line_peer}
         return [moved(partial.at[1 - core], core_in, {"tp": core_peer}, stage, 0)] + [
             moved(
-                partial.at[core, 1 - column, plane],
+                partial.at[(core, *spot(by_row, 1 - mine, part))],
                 row_in.at[step],
-                {"tp": row_peer},
+                peer,
                 stage,
                 1 + step,
             )
-            for step, plane in enumerate(order)
+            for step, part in enumerate(order)
         ]
 
-    def add_core(partial, core_in, steps, order):
+    def add_core(partial, core_in, steps, order, by_row):
+        mine = chosen(by_row)[0]
         steps[0].wait_recv()
-        for step, plane in enumerate(order):
-            total = partial[core, 1 - column, plane].astype(jnp.float32) + core_in[
-                1 - column, plane
-            ].astype(jnp.float32)
-            partial[core, 1 - column, plane] = total.astype(jnp.bfloat16)
+        for step, part in enumerate(order):
+            index = spot(by_row, 1 - mine, part)
+            total = partial[(core, *index)].astype(jnp.float32) + core_in[index].astype(jnp.float32)
+            partial[(core, *index)] = total.astype(jnp.bfloat16)
             steps[1 + step].start()
 
-    def add_row(partial, core_in, row_in, steps, step, plane):
+    def add_row(partial, core_in, row_in, steps, step, part, by_row):
+        index = spot(by_row, chosen(by_row)[0], part)
         steps[1 + step].wait_recv()
         return (
-            partial[core, column, plane].astype(jnp.float32)
-            + core_in[column, plane].astype(jnp.float32)
+            partial[(core, *index)].astype(jnp.float32)
+            + core_in[index].astype(jnp.float32)
             + row_in[step].astype(jnp.float32)
         )
 
+    ready(10)
     first = hand_over(gathered, 0)
-    ready(10)
+
     for step in (2, 1, 0):
         first[step].start()
-    launch(0)
-    launch(1)
-    launch(2)
-    launch(3)
+    for load, kinds in enumerate(((0,), (1,), (2, 3), (4, 5))):
+        ready(load)
+        for k in kinds:
+            launch(k)
+
     received(gathered, 0, 1).wait_recv()
     first[3].start()
+
     pump(0, sources[0])
+
     received(gathered, 0, 2).wait_recv()
     first[5].start()
     first[4].start()
+
     pump(0, sources[1])
+
     received(gathered, 0, 0).wait_recv()
     received(gathered, 0, 3).wait_recv()
+
     ready(11)
     normalize(gathered, input_gain, slot)
+
     pump(0, sources[2])
+
     received(gathered, 0, 5).wait_recv()
     first[6].start()
     received(gathered, 0, 4).wait_recv()
     received(gathered, 0, 6).wait_recv()
+
     normalize(gathered, input_gain, 1 - slot)
+
     ready(5)
     settle(0)
+
     for block in sources:
         pump(1, block)
+
     for plane in range(2):
         rows_out = jnp.dot(
             normed[plane], joined[...].reshape(width, 4 * group), preferred_element_type=jnp.float32
@@ -857,28 +883,37 @@
                 term = jnp.dot(rows_in[plane], weight[block], preferred_element_type=jnp.float32)
                 partial[side, x, plane] = term.astype(jnp.bfloat16)
 
-    steps = reducer(first_partial, first_core, first_row, 0) + [
+    steps = reducer(first_partial, first_core, first_row, 0, (0, 1), True) + [
         moved(first_partial.at[core, column, plane], first_line.at[plane], {"fs": line_peer}, 0, 3 + plane)
         for plane in range(2)
     ]
     fill(mixed, merge, first_partial, 1 - core)
     steps[0].start()
     fill(mixed, merge, first_partial, core)
-    add_core(first_partial, first_core, steps, (0, 1))
-    pump(2, others[0])
+
+    add_core(first_partial, first_core, steps, (0, 1), True)
+
+    for block in others:
+        pump(2, block)
+    pump(3, others[0])
     for plane in range(2):
-        total = add_row(first_partial, first_core, first_row, steps, plane, plane)
+        total = add_row(first_partial, first_core, first_row, steps, plane, plane, True)
         first_partial[core, column, plane] = total.astype(jnp.bfloat16)
         steps[3 + plane].start()
+
     ready(4)
     for i in range(pieces):
         for there in others:
-            post(4 + i, there).start()
+            post(first_down + i, there).start()
 
     second = [share_mid(step) for step in range(6)]
-    pump(2, others[1])
-    pump(2, others[2])
-    pump(3, others[0])
+
+    pump(3, others[1])
+    pump(3, others[2])
+
+    for block in others:
+        pump(4, block)
+    pump(5, others[0])
     for plane in range(2):
         steps[3 + plane].wait_recv()
         total = gathered[plane, seat].astype(jnp.float32) + (
@@ -888,8 +923,8 @@
         gathered_mid[plane, seat] = total.astype(jnp.bfloat16)
         second[plane].start()
         second[2 + plane].start()
-        pump(3, others[1 + plane])
-    queue = [(4 + i, block) for i in range(pieces) for block in others]
+        pump(5, others[1 + plane])
+    queue = [(first_down + i, block) for i in range(pieces) for block in [line_peer] + crossing]
 
     def pump_next(count):
         for _ in range(count):
@@ -903,10 +938,11 @@
         shared_mid(2 + plane).wait_recv()
         shared_mid(4 + plane).wait_recv()
         normalize(gathered_mid, middle_gain, plane)
+
     ready(7)
     ready(8)
-    settle(2)
-    settle(3)
+    for k in range(2, first_down):
+        settle(k)
     tile = 256
     for plane in range(2):
         for begin in range(0, hidden_half, tile):
@@ -922,29 +958,47 @@
             hidden[plane, :, columns] = (gate_act / (1.0 + jnp.exp(-gate_act)) * up_act).astype(
                 jnp.bfloat16
             )
-        if plane == 0:
-            pump_next(len(others))
+            if plane == 0:
+                pump_next(1)
+
+    pump_next(1)
 
     ready(9)
-    ends = [
-        reducer(last_partial.at[i], last_core.at[i], last_row.at[i], 1 + i)
-        + [
-            moved(
-                last_partial.at[i, core, column, 1 - slot],
-                last_line.at[i],
-                {"fs": line_peer},
+    by_rows = [i in (0, 2) for i in range(pieces)]
+    ends = []
+    for i in range(pieces):
+        mine, other = chosen(by_rows[i])
+        ends.append(
+            reducer(
+                last_partial.at[i],
+                last_core.at[i],
+                last_row.at[i],
                 1 + i,
-                3,
+                (1 - other, other),
+                by_rows[i],
             )
-        ]
-        for i in range(pieces)
-    ]
+            + [
+                moved(
+                    last_partial.at[(i, core, *spot(by_rows[i], mine, 1 - other))],
+                    last_line.at[i],
+                    {"fs": line_peer} if by_rows[i] else {"tp": row_peer},
+                    1 + i,
+                    3,
+                )
+            ]
+        )
+
+    def last_sum(i, step):
+        other = chosen(by_rows[i])[1]
+        part = other if step else 1 - other
+        return add_row(
+            last_partial.at[i], last_core.at[i], last_row.at[i], ends[i], step, part, by_rows[i]
+        )
 
     def pass_line(i):
-        total = add_row(
-            last_partial.at[i], last_core.at[i], last_row.at[i], ends[i], 0, 1 - slot
-        )
-        last_partial[i, core, column, 1 - slot] = total.astype(jnp.bfloat16)
+        total = last_sum(i, 0)
+        mine, other = chosen(by_rows[i])
+        last_partial[(i, core, *spot(by_rows[i], mine, 1 - other))] = total.astype(jnp.bfloat16)
         ends[i][3].start()
 
     written = [
@@ -958,27 +1012,28 @@
 
     def finish(i):
         span = slice(i * piece_width, (i + 1) * piece_width)
-        total = gathered_mid[slot, seat, :, span].astype(jnp.float32) + add_row(
-            last_partial.at[i], last_core.at[i], last_row.at[i], ends[i], 1, slot
-        )
+        total = gathered_mid[slot, seat, :, span].astype(jnp.float32) + last_sum(i, 1)
         ends[i][3].wait_recv()
         finished[:, span] = (total + last_line[i].astype(jnp.float32)).astype(jnp.bfloat16)
         written[i].start()
 
     for i in range(pieces):
-        if i == 2:
-            pump_next(len(queue))
-        settle(4 + i)
+        settle(first_down + i)
         fill(hidden, down.at[i], last_partial.at[i], 1 - core)
         ends[i][0].start()
+        if queue:
+            pump_next(1)
         fill(hidden, down.at[i], last_partial.at[i], core)
-        add_core(last_partial.at[i], last_core.at[i], ends[i], (1 - slot, slot))
-        if i:
-            pass_line(i - 1)
+        if queue:
+            pump_next(1)
+        other = chosen(by_rows[i])[1]
+        add_core(last_partial.at[i], last_core.at[i], ends[i], (1 - other, other), by_rows[i])
         if i > 1:
-            finish(i - 2)
-    pass_line(pieces - 1)
+            pass_line(i - 2)
     for i in range(max(0, pieces - 2), pieces):
+        pass_line(i)
+
+    for i in range(pieces):
         finish(i)
 
     for copy in written:
@@ -988,7 +1043,7 @@
     for group_steps in ends:
         for copy in group_steps:
             copy.wait_send()
-    for k in range(4 + pieces):
+    for k in range(first_down + pieces):
         for there in others:
             post(k, there).wait_send()
             across(k, there, half).wait_send()
@@ -1004,7 +1059,7 @@
     hidden_half, group = gate_weight.shape[1] // 2, ret_width // 2
     pieces = 4
     piece_width = down_weight.shape[1] // pieces
-    kinds = 4 + pieces
+    kinds = 6 + pieces
     anywhere = pl.BlockSpec(memory_space=pl.ANY)
     in_smem = pl.BlockSpec(memory_space=pltpu.SMEM)
 

time: 144 us -> 141 us (0.979)
  Pallas kernels: 142 us -> 139 us
    pallas_call x1, Pallas kernels: 142 us -> 139 us  [paired_call(): pl.pallas_call(functools.partial(paired_kernel, sizes), out_shape=jax.Sha...]
where the time goes in v5:
time: 141 us
  Pallas kernels  139 us (99%)
  local copies, waits for them, and re-layouts  1.77 us (1%)
    pallas_call x1, Pallas kernels, paired_call(): pl.pallas_call(functools.partial(paired_kernel, sizes), out_shape=jax.Sha...  139 us

profile of v5, /device:TPU:0, one launch (start us, length us, event | category | flops | bytes accessed | tf_op | source)
XLA Modules:
  0.0 141.1 jit_solution(7146567091232998426)
XLA Ops:
  0.0 139.3 %shard_map.145 = bf16[384,512]{1,0:T(8,128)(2,1)} custom-call(bf16[384,512]{1,0:T(8,128)(2,1)} %bitcast.5, f32[1,2048]{1,0:T(1,128)} %bitcast.6, f32[1,2048]{1,0:T(1,128)} %bitcast.7, f32[4]{0:T(128)} %ahead.1, f32[4]{0:T(128)} %behind.1, f32[384,128]{1,0:T(8,128)} %constant.4.clone.cosine_in, f32[384,128]{1,0:T(8,128)} %constant.5.clone.sine_in, ...), custom_call_target="tpu_custom_call" | custom-call | tf_op jit(solution)/shard_map/pallas_call | solution.py:1075
  139.3 1.8 %copy.17 = bf16[1,384,512]{2,1,0:T(8,128)(2,1)} copy(bf16[1,384,512]{2,1,0:T(8,128)(2,1)} %bitcast.4) | data formatting | bytes 786432

commit v6 on v5

--- a/solution.py
+++ b/solution.py
@@ -561,11 +561,9 @@
         for source, target in pairs:
             own[-1].append(pltpu.make_async_copy(source, target, own_sem.at[index]))
             index += 1
-
     for copies in (own[-2], *own[:-2], own[-1]):
         for copy in copies:
             copy.start()
-
     pl.semaphore_wait(barrier, line - 1 + 1 + 2)
 
     def ready(k):
@@ -761,46 +759,33 @@
 
     ready(10)
     first = hand_over(gathered, 0)
-
     for step in (2, 1, 0):
         first[step].start()
     for load, kinds in enumerate(((0,), (1,), (2, 3), (4, 5))):
         ready(load)
         for k in kinds:
             launch(k)
-
     received(gathered, 0, 1).wait_recv()
     first[3].start()
-
     pump(0, sources[0])
-
     received(gathered, 0, 2).wait_recv()
     first[5].start()
     first[4].start()
-
     pump(0, sources[1])
-
     received(gathered, 0, 0).wait_recv()
     received(gathered, 0, 3).wait_recv()
-
     ready(11)
     normalize(gathered, input_gain, slot)
-
     pump(0, sources[2])
-
     received(gathered, 0, 5).wait_recv()
     first[6].start()
     received(gathered, 0, 4).wait_recv()
     received(gathered, 0, 6).wait_recv()
-
     normalize(gathered, input_gain, 1 - slot)
-
     ready(5)
     settle(0)
-
     for block in sources:
         pump(1, block)
-
     for plane in range(2):
         rows_out = jnp.dot(
             normed[plane], joined[...].reshape(width, 4 * group), preferred_element_type=jnp.float32
@@ -890,9 +875,7 @@
     fill(mixed, merge, first_partial, 1 - core)
     steps[0].start()
     fill(mixed, merge, first_partial, core)
-
     add_core(first_partial, first_core, steps, (0, 1), True)
-
     for block in others:
         pump(2, block)
     pump(3, others[0])
@@ -900,17 +883,14 @@
         total = add_row(first_partial, first_core, first_row, steps, plane, plane, True)
         first_partial[core, column, plane] = total.astype(jnp.bfloat16)
         steps[3 + plane].start()
-
     ready(4)
     for i in range(pieces):
         for there in others:
             post(first_down + i, there).start()
 
     second = [share_mid(step) for step in range(6)]
-
     pump(3, others[1])
     pump(3, others[2])
-
     for block in others:
         pump(4, block)
     pump(5, others[0])
@@ -930,21 +910,7 @@
         for _ in range(count):
             pump(*queue.pop(0))
 
-    for plane in range(2):
-        shared_mid(plane).wait_recv()
-        second[4 + plane].start()
-        pump_next(len(others))
-    for plane in range(2):
-        shared_mid(2 + plane).wait_recv()
-        shared_mid(4 + plane).wait_recv()
-        normalize(gathered_mid, middle_gain, plane)
-
-    ready(7)
-    ready(8)
-    for k in range(2, first_down):
-        settle(k)
-    tile = 256
-    for plane in range(2):
+    def product(plane):
         for begin in range(0, hidden_half, tile):
             columns = slice(begin, min(begin + tile, hidden_half))
             gate_act, up_act = [
@@ -958,11 +924,28 @@
             hidden[plane, :, columns] = (gate_act / (1.0 + jnp.exp(-gate_act)) * up_act).astype(
                 jnp.bfloat16
             )
-            if plane == 0:
+            if plane == 1:
                 pump_next(1)
 
-    pump_next(1)
-
+    tile = 256
+    shared_mid(0).wait_recv()
+    second[4].start()
+    pump_next(len(others))
+    shared_mid(2).wait_recv()
+    shared_mid(4).wait_recv()
+    normalize(gathered_mid, middle_gain, 0)
+    ready(7)
+    ready(8)
+    for k in range(2, first_down):
+        settle(k)
+    product(0)
+    shared_mid(1).wait_recv()
+    second[5].start()
+    pump_next(len(others))
+    shared_mid(3).wait_recv()
+    shared_mid(5).wait_recv()
+    normalize(gathered_mid, middle_gain, 1)
+    product(1)
     ready(9)
     by_rows = [i in (0, 2) for i in range(pieces)]
     ends = []
@@ -1021,18 +1004,15 @@
         settle(first_down + i)
         fill(hidden, down.at[i], last_partial.at[i], 1 - core)
         ends[i][0].start()
-        if queue:
-            pump_next(1)
         fill(hidden, down.at[i], last_partial.at[i], core)
-        if queue:
-            pump_next(1)
         other = chosen(by_rows[i])[1]
         add_core(last_partial.at[i], last_core.at[i], ends[i], (1 - other, other), by_rows[i])
+        if queue:
+            pump_next(1 if i == 0 else 2)
         if i > 1:
             pass_line(i - 2)
     for i in range(max(0, pieces - 2), pieces):
         pass_line(i)
-
     for i in range(pieces):
         finish(i)
 

time: 141 us -> 139 us (0.986)
  Pallas kernels: 139 us -> 137 us
    pallas_call x1, Pallas kernels: 139 us -> 137 us  [paired_call(): pl.pallas_call(functools.partial(paired_kernel, sizes), out_shape=jax.Sha...]
where the time goes in v6:
time: 139 us
  Pallas kernels  137 us (99%)
  local copies, waits for them, and re-layouts  1.77 us (1%)
    pallas_call x1, Pallas kernels, paired_call(): pl.pallas_call(functools.partial(paired_kernel, sizes), out_shape=jax.Sha...  137 us

profile of v6, /device:TPU:0, one launch (start us, length us, event | category | flops | bytes accessed | tf_op | source)
XLA Modules:
  0.0 138.9 jit_solution(13152015505533234104)
XLA Ops:
  0.0 137.1 %shard_map.145 = bf16[384,512]{1,0:T(8,128)(2,1)} custom-call(bf16[384,512]{1,0:T(8,128)(2,1)} %bitcast.5, f32[1,2048]{1,0:T(1,128)} %bitcast.6, f32[1,2048]{1,0:T(1,128)} %bitcast.7, f32[4]{0:T(128)} %ahead.1, f32[4]{0:T(128)} %behind.1, f32[384,128]{1,0:T(8,128)} %constant.4.clone.cosine_in, f32[384,128]{1,0:T(8,128)} %constant.5.clone.sine_in, ...), custom_call_target="tpu_custom_call" | custom-call | tf_op jit(solution)/shard_map/pallas_call | solution.py:1055
  137.1 1.8 %copy.17 = bf16[1,384,512]{2,1,0:T(8,128)(2,1)} copy(bf16[1,384,512]{2,1,0:T(8,128)(2,1)} %bitcast.4) | data formatting | bytes 786432

commit v7 on v6

--- a/solution.py
+++ b/solution.py
@@ -1011,9 +1011,11 @@
             pump_next(1 if i == 0 else 2)
         if i > 1:
             pass_line(i - 2)
-    for i in range(max(0, pieces - 2), pieces):
-        pass_line(i)
-    for i in range(pieces):
+    pass_line(pieces - 2)
+    for i in range(pieces - 2):
+        finish(i)
+    pass_line(pieces - 1)
+    for i in range(pieces - 2, pieces):
         finish(i)
 
     for copy in written:

time: 139 us -> 141 us (1.014)
  Pallas kernels: 137 us -> 139 us
    pallas_call x1, Pallas kernels: 137 us -> 139 us  [paired_call(): pl.pallas_call(functools.partial(paired_kernel, sizes), out_shape=jax.Sha...]
where the time goes in v7:
time: 141 us; the launch traced here: 140 us
  Pallas kernels  139 us (99%)
  local copies, waits for them, and re-layouts  1.77 us (1%)
    pallas_call x1, Pallas kernels, paired_call(): pl.pallas_call(functools.partial(paired_kernel, sizes), out_shape=jax.Sha...  139 us

profile of v7, /device:TPU:0, one launch (start us, length us, event | category | flops | bytes accessed | tf_op | source)
XLA Modules:
  0.0 140.4 jit_solution(13712151820999394279)
XLA Ops:
  0.0 138.6 %shard_map.145 = bf16[384,512]{1,0:T(8,128)(2,1)} custom-call(bf16[384,512]{1,0:T(8,128)(2,1)} %bitcast.5, f32[1,2048]{1,0:T(1,128)} %bitcast.6, f32[1,2048]{1,0:T(1,128)} %bitcast.7, f32[4]{0:T(128)} %ahead.1, f32[4]{0:T(128)} %behind.1, f32[384,128]{1,0:T(8,128)} %constant.4.clone.cosine_in, f32[384,128]{1,0:T(8,128)} %constant.5.clone.sine_in, ...), custom_call_target="tpu_custom_call" | custom-call | tf_op jit(solution)/shard_map/pallas_call | solution.py:1057
  138.6 1.8 %copy.17 = bf16[1,384,512]{2,1,0:T(8,128)(2,1)} copy(bf16[1,384,512]{2,1,0:T(8,128)(2,1)} %bitcast.4) | data formatting | bytes 786432
